TPU v7x, 128 devices: a whole 4x4x4 slice. The times are simulated.
128 devices in a mesh: sp: 32 (over z, y, core), tp: 4 (over x).
Axes of the slice: x: 4, y: 4, z: 4, core: 2. Of those that a mesh axis runs over, the one named last changes fastest.
Arguments:
- stream: bfloat16 [16384, 2048], P(('sp', 'tp')), may hold values from -6 to 6
- conv_in_a: bfloat16 [16384, 1024], P('sp', 'tp'), may hold values from -6 to 6
- conv_in_b: bfloat16 [16384, 1024], P('sp', 'tp'), may hold values from -6 to 6
- gate_in_a: bfloat16 [16384, 1024], P('sp', 'tp'), may hold values from -6 to 6
- gate_in_b: bfloat16 [16384, 1024], P('sp', 'tp'), may hold values from -6 to 6
- conv_w_a: bfloat16 [4, 1024], P(None, 'tp'), may hold values from -3 to 3
- conv_w_b: bfloat16 [4, 1024], P(None, 'tp'), may hold values from -3 to 3
- rec_gate_a: bfloat16 [16, 64, 64], P('tp'), may hold values from -0.75 to 0.75
- inp_gate_a: bfloat16 [16, 64, 64], P('tp'), may hold values from -0.75 to 0.75
- rec_gate_b: bfloat16 [8, 128, 128], P('tp'), may hold values from -0.5 to 0.5
- inp_gate_b: bfloat16 [8, 128, 128], P('tp'), may hold values from -0.5 to 0.5
- decay_a: float32 [1024], P('tp'), may hold values from 3 to 20
- decay_b: float32 [1024], P('tp'), may hold values from 3 to 20
- decay_increments: float32 [16384], P('sp'), may hold values from -0.7 to 0
- out_w_a: bfloat16 [1024, 2048], P('tp'), may hold values from -0.5 to 0.5
- out_w_b: bfloat16 [1024, 2048], P('tp'), may hold values from -0.5 to 0.5
- norm_gain: bfloat16 [2048], replicated, may hold values from 0.099609375 to 1.8984375
- expert_ids: int32 [16384, 2], P(('sp', 'tp')), may hold values from 0 to 127, as said below
- group_prob: float32 [16384], P(('sp', 'tp')), may hold values from 0.3 to 1
- pick_gap: float32 [16384], P(('sp', 'tp')), may hold values from -6 to 6
- w_gate: bfloat16 [128, 2048, 1024], P(('sp', 'tp')), may hold values from -0.125 to 0.125
- w_up: bfloat16 [128, 2048, 1024], P(('sp', 'tp')), may hold values from -0.125 to 0.125
- w_down: bfloat16 [128, 1024, 2048], P(('sp', 'tp')), may hold values from -0.5 to 0.5
Outputs:
- result: bfloat16 [16384, 2048], P(('sp', 'tp'))
Inputs may be any that keep to these rules, and one draw needn't show every extreme that they name: `expert_ids`: each row names two different experts of one group: both lie in g * 32 to g * 32 + 31 for some g. In each aligned block of 128 rows no expert is named more than 4 times, and in every block some expert is named exactly 4 times.
All inputs are finite; a program needn't handle non-finite values.
Results may differ from a plain program's by a relative error of at most 0.015.
Values may be sent and summed in bfloat16 or wider, within the bound.
A program may use at most 128 MiB of HBM per device.

v0:
```python
import jax
import jax.numpy as jnp
from jax import lax
from jax.sharding import PartitionSpec as P

EPSILON = 1e-06
GATE_SCALE = 8.0


def from_behind(array, axis, by):
    size = lax.axis_size(axis)
    pairs = [(i, i + by) for i in range(size) if 0 <= i + by < size]
    return lax.ppermute(array, axis, pairs)


def from_everyone(array, axis):
    size = lax.axis_size(axis)
    return lax.all_to_all(
        jnp.broadcast_to(array[None], (size, *array.shape)), axis, 0, 0, tiled=True
    )


def gathered_once(array, axis):
    leaves = jax.tree.leaves(array)
    turns = sorted(range(len(leaves)), key=lambda k: -leaves[k].size)
    width = (1, *leaves[turns[0]].shape)[-1]
    lines = [
        jnp.pad(leaves[k].reshape(-1), (0, -leaves[k].size % width)).reshape(-1, width)
        for k in turns
    ]
    both, at, found = (from_everyone(jnp.concatenate(lines), axis), 0, {})
    for k, line in zip(turns, lines):
        slab = both[:, at : at + len(line)].reshape(len(both), -1)
        found[k] = slab[:, : leaves[k].size].reshape(-1, *leaves[k].shape)
        at += len(line)
    numbers = iter(range(len(leaves)))
    return jax.tree.map(lambda _: found[next(numbers)], array)


def folded_in_pairs(pieces, combine):
    while len(jax.tree.leaves(pieces)[0]) > 1:
        pieces = jax.vmap(combine)(
            *(jax.tree.map(lambda part: part[side::2], pieces) for side in (0, 1))
        )
    return jax.tree.map(lambda part: part[0], pieces)


def carried_in(array, axis, combine, identity):
    size, position = (lax.axis_size(axis), lax.axis_index(axis))
    passed = jnp.arange(size) < position

    def kept(part, zero, own):
        part = jnp.where(
            passed.reshape(-1, *(1 for _ in own.shape)), part, jnp.asarray(zero, own.dtype)
        )
        return part

    pieces = gathered_once(array, axis)
    return folded_in_pairs(jax.tree.map(kept, pieces, identity, array), combine)


def split_up(array, dim, size):
    before, after = (array.shape[:dim], array.shape[dim + 1 :])
    return jnp.moveaxis(array.reshape(*before, size, -1, *after), dim, 0)


def sum_at_owner(array, axis, dim):
    pieces = split_up(array, dim, lax.axis_size(axis))
    arrived = lax.all_to_all(pieces, axis, split_axis=0, concat_axis=0, tiled=True)
    return arrived.astype(jnp.float32).sum(axis=0)


def causal_taps(source, tail_rows, weights):
    length = source.shape[0]
    tap_count = weights.shape[0]
    rim_count = tail_rows.shape[0]
    row_index = jnp.arange(length, dtype=jnp.int32)[:, None]
    own_index = jnp.arange(length, dtype=jnp.int32)[None, :]
    rim_index = jnp.arange(rim_count, dtype=jnp.int32)[None, :]
    total = weights[tap_count - 1].astype(jnp.float32)[None, :] * source.astype(jnp.float32)
    for offset in range(tap_count - 1):
        lag = tap_count - 1 - offset
        own_shift = (row_index - own_index == lag).astype(jnp.bfloat16)
        rim_shift = (rim_index == rim_count + row_index - lag).astype(jnp.bfloat16)
        moved = jnp.dot(own_shift, source, preferred_element_type=jnp.float32)
        moved = moved + jnp.dot(rim_shift, tail_rows, preferred_element_type=jnp.float32)
        total = total + weights[offset].astype(jnp.float32)[None, :] * moved
    return total.astype(jnp.bfloat16)


def recurrence_inputs(conv_out, rec_gate, inp_gate, decay, jump_log):
    length = conv_out.shape[0]
    head_count = rec_gate.shape[0]
    head_dim = rec_gate.shape[1]
    blocks = conv_out.reshape(length, head_count, head_dim)
    recur = jax.nn.sigmoid(
        jnp.einsum("thi,hij->thj", blocks, rec_gate, preferred_element_type=jnp.float32).reshape(
            length, -1
        )
    )
    admit = jax.nn.sigmoid(
        jnp.einsum("thi,hij->thj", blocks, inp_gate, preferred_element_type=jnp.float32).reshape(
            length, -1
        )
    )
    log_decay = -GATE_SCALE * recur * jax.nn.softplus(-decay)[None, :] + jump_log[:, None]
    drive = jnp.sqrt(-jnp.expm1(2.0 * log_decay)) * admit * conv_out.astype(jnp.float32)
    return (log_decay, drive)


def link_states(earlier, later):
    return (earlier[0] * later[0], later[0] * earlier[1] + later[1])


def local_recurrence(log_decay, drives):
    length, channel_count = log_decay.shape
    span = min(128, length)
    block_count = length // span
    lower = jnp.arange(span, dtype=jnp.int32)[:, None] >= jnp.arange(span, dtype=jnp.int32)[None, :]
    cumulative = jnp.einsum(
        "ts,bsc->btc",
        lower.astype(jnp.float32),
        log_decay.reshape(block_count, span, channel_count),
        precision=lax.Precision.HIGHEST,
    )
    drive_blocks = drives.reshape(block_count, span, channel_count)

    def block_states(operands):
        cum_block, drive_block = operands
        spread = jnp.minimum(cum_block[:, None, :] - cum_block[None, :, :], 0.0)
        weight = jnp.where(lower[:, :, None], jnp.exp(spread), 0.0)
        return jnp.sum(weight * drive_block[None, :, :], axis=1)

    inner_states = lax.map(block_states, (cumulative, drive_blocks))
    within_factor = jnp.exp(cumulative)

    def link_blocks(carry, operands):
        factor_end, state_end = operands
        carry_factor, carry_state = carry
        following = (carry_factor * factor_end, factor_end * carry_state + state_end)
        return (following, carry)

    start_pair = (jnp.ones((channel_count,), jnp.float32), jnp.zeros((channel_count,), jnp.float32))
    last_pair, entering = lax.scan(
        link_blocks, start_pair, (within_factor[:, -1], inner_states[:, -1])
    )
    states = inner_states + within_factor * entering[1][:, None, :]
    running_factor = within_factor * entering[0][:, None, :]
    return (running_factor.reshape(length, channel_count), states.reshape(length, channel_count))


def shards(
    stream,
    conv_in_a,
    conv_in_b,
    gate_in_a,
    gate_in_b,
    conv_w_a,
    conv_w_b,
    rec_gate_a,
    inp_gate_a,
    rec_gate_b,
    inp_gate_b,
    decay_a,
    decay_b,
    decay_increments,
    out_w_a,
    out_w_b,
    norm_gain,
    expert_ids,
    group_prob,
    pick_gap,
    w_gate,
    w_up,
    w_down,
):
    tap_count = conv_w_a.shape[0]
    length = conv_in_a.shape[0]
    tail_a, tail_b = from_behind(
        (conv_in_a[length - tap_count + 1 :], conv_in_b[length - tap_count + 1 :]), "sp", 1
    )
    conv_a = causal_taps(conv_in_a, tail_a, conv_w_a)
    conv_b = causal_taps(conv_in_b, tail_b, conv_w_b)
    log_a, drive_a = recurrence_inputs(conv_a, rec_gate_a, inp_gate_a, decay_a, decay_increments)
    log_b, drive_b = recurrence_inputs(conv_b, rec_gate_b, inp_gate_b, decay_b, decay_increments)
    log_all = jnp.concatenate([log_a, log_b], axis=1)
    drives = jnp.concatenate([drive_a, drive_b], axis=1)
    running_factor, local_states = local_recurrence(log_all, drives)
    channel_count = log_all.shape[1]
    identity_pair = (
        jnp.ones((channel_count,), jnp.float32),
        jnp.zeros((channel_count,), jnp.float32),
    )
    incoming_factor, carried = carried_in(
        (running_factor[-1], local_states[-1]), "sp", link_states, identity_pair
    )
    states = local_states + running_factor * carried[None, :]
    width_a = conv_in_a.shape[1]
    hidden_a = (states[:, :width_a] * jax.nn.gelu(gate_in_a.astype(jnp.float32))).astype(
        jnp.bfloat16
    )
    hidden_b = (states[:, width_a:] * jax.nn.gelu(gate_in_b.astype(jnp.float32))).astype(
        jnp.bfloat16
    )
    tp_count = lax.axis_size("tp")
    row_count = length // tp_count
    part_a = jnp.dot(hidden_a, out_w_a, preferred_element_type=jnp.float32)
    part_b = jnp.dot(hidden_b, out_w_b, preferred_element_type=jnp.float32)
    mixed_rows = sum_at_owner((part_a + part_b).astype(jnp.bfloat16), "tp", 0)
    middle = (stream.astype(jnp.float32) + mixed_rows).astype(jnp.bfloat16)
    middle_f = middle.astype(jnp.float32)
    scale_rows = lax.rsqrt(jnp.mean(middle_f * middle_f, axis=-1, keepdims=True) + EPSILON)
    normed = (middle_f * scale_rows * norm_gain.astype(jnp.float32)[None, :]).astype(jnp.bfloat16)
    width = normed.shape[1]
    sequence_parallel_count = lax.axis_size("sp")
    experts = sequence_parallel_count * tp_count * w_gate.shape[0]
    slot_count = 4 * row_count // experts
    flat_ids = expert_ids.reshape(-1)
    onehot = (flat_ids[:, None] == jnp.arange(experts, dtype=jnp.int32)[None, :]).astype(jnp.int32)
    ranks = jnp.sum(jnp.cumsum(onehot, axis=0) * onehot, axis=1) - 1
    destination = flat_ids * slot_count + ranks
    copies = jnp.repeat(normed, expert_ids.shape[1], axis=0)
    buffer = jnp.zeros((experts * slot_count, width), jnp.bfloat16).at[destination].set(copies)
    buffer = buffer.reshape(experts, slot_count, width)
    arrived = lax.all_to_all(buffer, ("sp", "tp"), split_axis=0, concat_axis=0, tiled=True)
    flat_rows = arrived.reshape(-1, arrived.shape[-1])
    gate_part = jnp.dot(flat_rows, w_gate[0], preferred_element_type=jnp.float32)
    up_part = jnp.dot(flat_rows, w_up[0], preferred_element_type=jnp.float32)
    inner = (jax.nn.silu(gate_part) * up_part).astype(jnp.bfloat16)
    served = jnp.dot(inner, w_down[0], preferred_element_type=jnp.float32).astype(jnp.bfloat16)
    returned = lax.all_to_all(
        served.reshape(arrived.shape), ("sp", "tp"), split_axis=0, concat_axis=0, tiled=True
    )
    returned = returned.reshape(experts * slot_count, width)
    picked = returned[destination].reshape(row_count, expert_ids.shape[1], width)
    first_weight = group_prob * jax.nn.sigmoid(pick_gap)
    second_weight = group_prob * jax.nn.sigmoid(-pick_gap)
    total = (
        middle_f
        + first_weight[:, None] * picked[:, 0].astype(jnp.float32)
        + second_weight[:, None] * picked[:, 1].astype(jnp.float32)
    )
    return total.astype(jnp.bfloat16)


def solution(mesh):
    placed = (
        P(("sp", "tp"), None),
        P("sp", "tp"),
        P("sp", "tp"),
        P("sp", "tp"),
        P("sp", "tp"),
        P(None, "tp"),
        P(None, "tp"),
        P("tp", None, None),
        P("tp", None, None),
        P("tp", None, None),
        P("tp", None, None),
        P("tp"),
        P("tp"),
        P("sp"),
        P("tp", None),
        P("tp", None),
        P(),
        P(("sp", "tp"), None),
        P(("sp", "tp")),
        P(("sp", "tp")),
        P(("sp", "tp"), None, None),
        P(("sp", "tp"), None, None),
        P(("sp", "tp"), None, None),
    )
    return jax.shard_map(
        shards, mesh=mesh, in_specs=placed, out_specs=P(("sp", "tp"), None), check_vma=False
    )
```

profile of v0, /device:TPU:1, one launch (start us, length us, event | category | flops | bytes accessed | tf_op | source)
XLA Modules:
  0.0 241.2 jit_solution(13974527144673952250)
XLA Ops:
  0.0 0.8 slice.133
  0.8 4.6 %collective-permute-start.1 = (bf16[3,256]{1,0:T(4,128)(2,1)S(1)}, bf16[3,256]{1,0:T(4,128)(2,1)S(1)}, u32[]{:S(2)}, u32[]{:S(2)}) collective-permute-start(bf16[3,256]{1,0:T(4,128)(2,1)S(1)} %slice.133), channel_id=1, source_target_pairs={{0,4},{4,8},{8,12},{12,16},{16,20},{20,24},{24,28},{28,32},{32,36}... | collective-permute-start | bytes 4616 | tf_op jit(solution)/shard_map/ppermute | solution.py:13
  5.4 0.7 slice.128
  6.1 1.9 collective-permute-start
  8.0 2.1 fusion.52
  10.1 2.1 fusion.56
  12.2 1.4 fusion.60
  13.6 0.3 fusion.54
  13.9 1.1 fusion.58
  15.1 0.3 fusion.62
  15.9 1.3 fusion.21
  17.3 1.4 fusion.19
  18.7 0.4 fusion.38
  20.1 0.6 copy-done.12
  20.7 0.3 fusion.26
  21.1 0.4 fusion.37
  21.5 0.3 fusion.30
  22.3 0.8 fusion.86
  23.6 1.3 div.51
  24.9 1.0 copy.83
  26.3 1.2 multiply_add_fusion.4
  27.5 1.8 fusion.144
  29.3 42.3 %while.28 = (s32[]{:T(128)}, f32[4,128,512]{2,1,0:T(8,128)}, f32[4,128,512]{2,1,0:T(8,128)S(1)}, f32[4,128,512]{2,1,0:T(8,128)S(1)}, s32[]{:T(128)}) while((s32[]{:T(128)}, f32[4,128,512]{2,1,0:T(8,128)}, f32[4,128,512]{2,1,0:T(8,128)S(1)}, f32[4,128,512]{2,1,0:T(8,128)S(1)}, s32[]{:T(128)}) %tuple.79), condition=%wide.region_2.3_spmd.clone, body=%wide.region_0.2_spmd.clone.sunk | while | flops 41893888 | bytes 2392641 | solution.py:134
  29.3 9.8 %multiply_reduce_fusion.2 = f32[128,512]{1,0:T(8,128)S(1)} fusion(f32[128,512]{1,0:T(8,128)S(1)} %get-tuple-element.258, f32[128,512]{1,0:T(8,128)S(1)} %get-tuple-element.259, pred[128,128]{1,0:T(8,128)(4,1)S(1)} %iota_compare_fusion.14), kind=kLoop, calls=%fused_computation.3.clone.1 | loop fusion | flops 41877504 | bytes 802816 | tf_op jit(solution)/shard_map/while/body/eval_jaxpr/reduce_sum | solution.py:132
  39.1 0.7 bitcast_dynamic-update-slice_fusion.2
  39.9 9.8 %multiply_reduce_fusion.2 = f32[128,512]{1,0:T(8,128)S(1)} fusion(f32[128,512]{1,0:T(8,128)S(1)} %get-tuple-element.258, f32[128,512]{1,0:T(8,128)S(1)} %get-tuple-element.259, pred[128,128]{1,0:T(8,128)(4,1)S(1)} %iota_compare_fusion.14), kind=kLoop, calls=%fused_computation.3.clone.1 | loop fusion | flops 41877504 | bytes 802816 | tf_op jit(solution)/shard_map/while/body/eval_jaxpr/reduce_sum | solution.py:132
  49.7 0.7 bitcast_dynamic-update-slice_fusion.2
  50.5 9.8 %multiply_reduce_fusion.2 = f32[128,512]{1,0:T(8,128)S(1)} fusion(f32[128,512]{1,0:T(8,128)S(1)} %get-tuple-element.258, f32[128,512]{1,0:T(8,128)S(1)} %get-tuple-element.259, pred[128,128]{1,0:T(8,128)(4,1)S(1)} %iota_compare_fusion.14), kind=kLoop, calls=%fused_computation.3.clone.1 | loop fusion | flops 41877504 | bytes 802816 | tf_op jit(solution)/shard_map/while/body/eval_jaxpr/reduce_sum | solution.py:132
  60.3 0.7 bitcast_dynamic-update-slice_fusion.2
  61.1 9.8 %multiply_reduce_fusion.2 = f32[128,512]{1,0:T(8,128)S(1)} fusion(f32[128,512]{1,0:T(8,128)S(1)} %get-tuple-element.258, f32[128,512]{1,0:T(8,128)S(1)} %get-tuple-element.259, pred[128,128]{1,0:T(8,128)(4,1)S(1)} %iota_compare_fusion.14), kind=kLoop, calls=%fused_computation.3.clone.1 | loop fusion | flops 41877504 | bytes 802816 | tf_op jit(solution)/shard_map/while/body/eval_jaxpr/reduce_sum | solution.py:132
  70.8 0.7 bitcast_dynamic-update-slice_fusion.2
  71.6 1.9 copy.88
  73.5 0.8 slice.169
  74.3 0.6 while.29
  75.0 1.5 broadcast_multiply_fusion
  76.5 0.9 copy-done.4
  77.5 0.7 broadcast_in_dim.49
  78.2 8.3 %all-to-all-start = ((f32[32,2,512]{2,1,0:T(2,128)}), f32[32,2,512]{2,1,0:T(2,128)S(1)}, u32[]{:S(2)}, u32[]{:S(2)}) async-start(f32[32,2,512]{2,1,0:T(2,128)} %broadcast_in_dim.49), calls=%async_computation | async-start | bytes 262144 | tf_op jit(solution)/shard_map/all_to_all | solution.py:18
  86.5 7.6 %all-to-all-done = f32[32,2,512]{2,1,0:T(2,128)S(1)} async-done(((f32[32,2,512]{2,1,0:T(2,128)}), f32[32,2,512]{2,1,0:T(2,128)S(1)}, u32[]{:S(2)}, u32[]{:S(2)}) %all-to-all-start) | async-done | bytes 131104 | tf_op jit(solution)/shard_map/all_to_all | solution.py:18
  94.3 0.6 slice.141
  94.9 0.6 slice.142
  95.6 0.8 fusion.141
  97.0 0.8 fusion.99
  97.8 0.4 copy-done.10
  98.2 2.2 add_convert_fusion
  100.4 4.1 %all-to-all-start.1 = ((bf16[4,128,2048]{2,1,0:T(8,128)(2,1)}), bf16[4,128,2048]{2,1,0:T(8,128)(2,1)S(1)}, u32[]{:S(2)}, u32[]{:S(2)}) async-start(bf16[4,128,2048]{2,1,0:T(8,128)(2,1)} %bitcast.168), calls=%async_computation.1 | async-start | bytes 4194304 | tf_op jit(solution)/shard_map/all_to_all | solution.py:69
  105.9 24.4 %all-to-all-done.1 = bf16[4,128,2048]{2,1,0:T(8,128)(2,1)S(1)} async-done(((bf16[4,128,2048]{2,1,0:T(8,128)(2,1)}), bf16[4,128,2048]{2,1,0:T(8,128)(2,1)S(1)}, u32[]{:S(2)}, u32[]{:S(2)}) %all-to-all-start.1) | async-done | bytes 2097184 | tf_op jit(solution)/shard_map/all_to_all | solution.py:69
  130.3 0.4 convert_reduce_fusion
  131.2 0.6 broadcast_in_dim.57
  131.8 1.2 reshape.238
  133.0 3.5 %scatter_custom_fusion = bf16[512,2048]{1,0:T(8,128)(2,1)S(1)} fusion(s32[256]{0:T(256)S(1)} %bitcast.192, bf16[256,2048]{1,0:T(8,128)(2,1)} %reshape.238, bf16[]{:T(256)} %constant.84.clone.1), kind=kCustom, calls=%fused_computation.74 | custom fusion | bytes 2097664 | tf_op jit(solution)/shard_map/scatter | solution.py:223
  136.5 2.2 reshape.211
  138.8 36.1 %all_to_all.20 = bf16[128,4,2048]{2,1,0:T(4,128)(2,1)S(1)} all-to-all(bf16[128,4,2048]{2,1,0:T(4,128)(2,1)} %reshape.211), channel_id=1, replica_groups=mesh['sp'=32,'tp'=4] {'sp','tp'}, dimensions={0} | all-to-all | bytes 4194304 | tf_op jit(solution)/shard_map/all_to_all | solution.py:225
  174.9 2.0 reshape.212
  176.9 6.7 %fusion.6 = f32[512,1024]{1,0:T(8,128)} fusion(bf16[512,2048]{1,0:T(8,128)(2,1)} %reshape.212, bf16[1,2048,1024]{2,1,0:T(8,128)(2,1)} %param.47), kind=kOutput, calls=%fused_computation.17 | convolution fusion | flops 2147483648 | bytes 8388608 | tf_op jit(solution)/shard_map/dot_general | solution.py:227
  183.6 9.9 %fusion.8 = bf16[512,2048]{1,0:T(8,128)(2,1)} fusion(bf16[1,1024,2048]{2,1,0:T(8,128)(2,1)} %param.49, f32[512,1024]{1,0:T(8,128)} %fusion.6, bf16[512,2048]{1,0:T(8,128)(2,1)S(1)} %copy-done.6, bf16[1,2048,1024]{2,1,0:T(8,128)(2,1)} %param.48), kind=kOutput, calls=%fused_computation.21 | convolution fusion | flops 4299161600 | bytes 14680064 | tf_op jit(solution)/shard_map/dot_general | solution.py:230
  193.5 4.1 %reshape.213 = bf16[128,4,2048]{2,1,0:T(4,128)(2,1)} reshape(bf16[512,2048]{1,0:T(8,128)(2,1)} %fusion.8) | data formatting | bytes 4194304 | tf_op jit(solution)/shard_map/reshape | solution.py:232
  197.6 5.0 %all-to-all-start.3 = ((bf16[128,4,2048]{2,1,0:T(4,128)(2,1)}), bf16[128,4,2048]{2,1,0:T(4,128)(2,1)}, u32[]{:S(2)}, u32[]{:S(2)}) async-start(bf16[128,4,2048]{2,1,0:T(4,128)(2,1)} %reshape.213), calls=%async_computation.3 | async-start | bytes 4194304 | tf_op jit(solution)/shard_map/all_to_all | solution.py:231
  202.7 30.5 %all-to-all-done.3 = bf16[128,4,2048]{2,1,0:T(4,128)(2,1)} async-done(((bf16[128,4,2048]{2,1,0:T(4,128)(2,1)}), bf16[128,4,2048]{2,1,0:T(4,128)(2,1)}, u32[]{:S(2)}, u32[]{:S(2)}) %all-to-all-start.3) | async-done | bytes 2097184 | tf_op jit(solution)/shard_map/all_to_all | solution.py:231
  233.2 2.5 %reshape.214 = bf16[512,2048]{1,0:T(8,128)(2,1)S(1)} reshape(bf16[128,4,2048]{2,1,0:T(4,128)(2,1)} %all-to-all-done.3) | data formatting | bytes 4194304 | tf_op jit(solution)/shard_map/reshape | solution.py:234
  235.7 1.4 gather_fusion
  237.1 0.7 reshape.215
  237.8 1.5 fusion.139
  239.3 1.9 fusion.43
  (153 shorter events, 5.9 us)
Async XLA Ops:
  0.0 96.9 %copy-start = (bf16[256,2048]{1,0:T(8,128)(2,1)S(1)}, bf16[256,2048]{1,0:T(8,128)(2,1)}, u32[]{:S(2)}) copy-start(bf16[256,2048]{1,0:T(8,128)(2,1)} %param.41) | copy-start | bytes 3145732
  0.0 13.6 %copy-start.14 = (bf16[512,256]{1,0:T(8,128)(2,1)S(1)}, bf16[512,256]{1,0:T(8,128)(2,1)}, u32[]{:S(2)}) copy-start(bf16[512,256]{1,0:T(8,128)(2,1)} %param.28) | copy-start | bytes 786436
  0.8 15.1 %collective-permute-start.1 = (bf16[3,256]{1,0:T(4,128)(2,1)S(1)}, bf16[3,256]{1,0:T(4,128)(2,1)S(1)}, u32[]{:S(2)}, u32[]{:S(2)}) collective-permute-start(bf16[3,256]{1,0:T(4,128)(2,1)S(1)} %slice.133), channel_id=1, source_target_pairs={{0,4},{4,8},{8,12},{12,16},{16,20},{20,24},{24,28},{28,32},{32,36}... | collective-permute-start | bytes 4616 | tf_op jit(solution)/shard_map/ppermute | solution.py:13
  6.1 13.8 %collective-permute-start = (bf16[3,256]{1,0:T(4,128)(2,1)S(1)}, bf16[3,256]{1,0:T(4,128)(2,1)S(1)}, u32[]{:S(2)}, u32[]{:S(2)}) collective-permute-start(bf16[3,256]{1,0:T(4,128)(2,1)S(1)} %slice.128), channel_id=1, source_target_pairs={{0,4},{4,8},{8,12},{12,16},{16,20},{20,24},{24,28},{28,32},{32,36}... | collective-permute-start | bytes 4616 | tf_op jit(solution)/shard_map/ppermute | solution.py:13
  12.2 3.3 %copy-start.17 = (bf16[4,256]{1,0:T(4,128)(2,1)S(1)}, bf16[4,256]{1,0:T(4,128)(2,1)}, u32[]{:S(2)}) copy-start(bf16[4,256]{1,0:T(4,128)(2,1)} %param.33) | copy-start | bytes 6148
  12.2 3.3 %copy-start.18 = (bf16[4,256]{1,0:T(4,128)(2,1)S(1)}, bf16[4,256]{1,0:T(4,128)(2,1)}, u32[]{:S(2)}) copy-start(bf16[4,256]{1,0:T(4,128)(2,1)} %param.32) | copy-start | bytes 6148
  12.2 3.3 %copy-start.22 = (f32[256]{0:T(256)S(1)}, f32[256]{0:T(256)}, u32[]{:S(2)}) copy-start(f32[256]{0:T(256)} %param.38) | copy-start | bytes 3076
  12.2 3.3 %copy-start.23 = (f32[256]{0:T(256)S(1)}, f32[256]{0:T(256)}, u32[]{:S(2)}) copy-start(f32[256]{0:T(256)} %param.39) | copy-start | bytes 3076
  12.2 3.3 %copy-start.13 = (bf16[512,256]{1,0:T(8,128)(2,1)S(1)}, bf16[512,256]{1,0:T(8,128)(2,1)}, u32[]{:S(2)}) copy-start(bf16[512,256]{1,0:T(8,128)(2,1)} %param.29) | copy-start | bytes 786436
  15.9 3.1 %copy-start.26 = (bf16[2,128,128]{2,1,0:T(8,128)(2,1)S(1)}, bf16[2,128,128]{2,1,0:T(8,128)(2,1)}, u32[]{:S(2)}) copy-start(bf16[2,128,128]{2,1,0:T(8,128)(2,1)} %param.36) | copy-start | bytes 196612
  18.7 0.8 copy-start.27
  19.5 2.8 %copy-start.7 = (f32[2,512,128]{1,2,0:T(8,128)}, f32[2,512,128]{1,2,0:T(8,128)S(1)}, u32[]{:S(2)}) copy-start(f32[2,512,128]{1,2,0:T(8,128)S(1)} %fusion.32) | copy-start | bytes 1572868
  19.5 1.2 copy-start.12
  19.9 1.6 copy-start.28
  21.1 0.8 copy-start.29
  21.5 0.8 copy-start.19
  21.9 1.2 copy-start.8
  23.6 2.3 copy-start.9
  76.5 1.0 copy-start.4
  77.5 19.2 %copy-start.5 = (f32[4,128,512]{2,1,0:T(8,128)S(1)}, f32[4,128,512]{2,1,0:T(8,128)}, u32[]{:S(2)}) copy-start(f32[4,128,512]{2,1,0:T(8,128)} %copy-done.4) | copy-start | bytes 3145732
  78.2 15.9 %all-to-all-start = ((f32[32,2,512]{2,1,0:T(2,128)}), f32[32,2,512]{2,1,0:T(2,128)S(1)}, u32[]{:S(2)}, u32[]{:S(2)}) async-start(f32[32,2,512]{2,1,0:T(2,128)} %broadcast_in_dim.49), calls=%async_computation | async-start | bytes 262144 | tf_op jit(solution)/shard_map/all_to_all | solution.py:18
  94.2 2.7 %copy-start.15 = (bf16[512,256]{1,0:T(8,128)(2,1)S(1)}, bf16[512,256]{1,0:T(8,128)(2,1)}, u32[]{:S(2)}) copy-start(bf16[512,256]{1,0:T(8,128)(2,1)} %param.30) | copy-start | bytes 786436
  96.9 1.2 copy-start.10
  96.9 1.3 copy-start.16
  100.4 4.1 %copy-start.20 = (s32[128,2]{0,1:T(2,128)S(1)}, s32[128,2]{0,1:T(2,128)}, u32[]{:S(2)}) copy-start(s32[128,2]{0,1:T(2,128)} %param.44) | copy-start | bytes 3076
  100.4 4.5 %copy-start.21 = (bf16[2048]{0:T(1024)(128)(2,1)S(1)}, bf16[2048]{0:T(1024)(128)(2,1)}, u32[]{:S(2)}) copy-start(bf16[2048]{0:T(1024)(128)(2,1)} %param.43) | copy-start | bytes 12292
  100.4 29.9 %all-to-all-start.1 = ((bf16[4,128,2048]{2,1,0:T(8,128)(2,1)}), bf16[4,128,2048]{2,1,0:T(8,128)(2,1)S(1)}, u32[]{:S(2)}, u32[]{:S(2)}) async-start(bf16[4,128,2048]{2,1,0:T(8,128)(2,1)} %bitcast.168), calls=%async_computation.1 | async-start | bytes 4194304 | tf_op jit(solution)/shard_map/all_to_all | solution.py:69
  105.1 25.6 %copy-start.11 = (bf16[128,2048]{1,0:T(8,128)(2,1)S(1)}, bf16[128,2048]{1,0:T(8,128)(2,1)}, u32[]{:S(2)}) copy-start(bf16[128,2048]{1,0:T(8,128)(2,1)} %param.27) | copy-start | bytes 1572868
  131.0 2.1 copy-start.2
  176.9 6.7 %copy-start.6 = (bf16[512,2048]{1,0:T(8,128)(2,1)S(1)}, bf16[512,2048]{1,0:T(8,128)(2,1)}, u32[]{:S(2)}) copy-start(bf16[512,2048]{1,0:T(8,128)(2,1)} %reshape.212) | copy-start | bytes 6291460
  197.6 5.0 %copy-start.24 = (f32[128]{0:T(128)S(1)}, f32[128]{0:T(128)}, u32[]{:S(2)}) copy-start(f32[128]{0:T(128)} %param.45) | copy-start | bytes 1540
  197.6 5.0 %copy-start.25 = (f32[128]{0:T(128)S(1)}, f32[128]{0:T(128)}, u32[]{:S(2)}) copy-start(f32[128]{0:T(128)} %param.46) | copy-start | bytes 1540
  197.6 35.5 %all-to-all-start.3 = ((bf16[128,4,2048]{2,1,0:T(4,128)(2,1)}), bf16[128,4,2048]{2,1,0:T(4,128)(2,1)}, u32[]{:S(2)}, u32[]{:S(2)}) async-start(bf16[128,4,2048]{2,1,0:T(4,128)(2,1)} %reshape.213), calls=%async_computation.3 | async-start | bytes 4194304 | tf_op jit(solution)/shard_map/all_to_all | solution.py:231
  237.8 1.5 copy-start.3
  237.8 3.4 %copy-start.1 = (bf16[256,2048]{1,0:T(8,128)(2,1)S(1)}, bf16[256,2048]{1,0:T(8,128)(2,1)}, u32[]{:S(2)}) copy-start(bf16[256,2048]{1,0:T(8,128)(2,1)} %param.41) | copy-start | bytes 3145732
where the time goes:
time: 242 us; the launch traced here: 241 us
  waiting for transfers between devices  62.5 us (26%)
  other arithmetic  47.2 us (20%)
  local copies, waits for them, and re-layouts  36.2 us (15%)
  blocking collectives  36.1 us (15%)
  matrix products  34.3 us (14%)
  starting transfers between devices  23.9 us (10%)
    reduce_sum x4, other arithmetic, block_states(): return jnp.sum(weight * drive_block[None, :, :], axis=1)  39.1 us
    all_to_all x1, blocking collectives, shards(): lax.all_to_all(buffer, ('sp', 'tp'), split_axis=0, concat_axis=0, tiled=T...  36.1 us
    all_to_all x1, waiting for transfers between devices, shards(): lax.all_to_all(served.reshape(arrived.shape), ('sp', 'tp'), split_axis=0,...  30.5 us
    all_to_all x1, waiting for transfers between devices, sum_at_owner(): lax.all_to_all(pieces, axis, split_axis=0, concat_axis=0, tiled=True)  24.4 us
    dot_general x1, matrix products, shards(): jnp.dot(inner, w_down[0], preferred_element_type=jnp.float32)  9.94 us
    all_to_all x1, starting transfers between devices, from_everyone(): lax.all_to_all(jnp.broadcast_to(array[None], (size, *array.shape)), axis,...  8.32 us
    all_to_all x1, waiting for transfers between devices, from_everyone(): lax.all_to_all(jnp.broadcast_to(array[None], (size, *array.shape)), axis,...  7.58 us
    dot_general x6, matrix products, causal_taps(): moved = jnp.dot(own_shift, source, preferred_element_type=jnp.float32)  7.39 us
  transfers between devices with their start and end apart: 5, of which 3 were waited for; matrix products, arithmetic and copies ran while one was open for 6% of the time, Pallas kernels for 0%

commit v1 on v0

v1 whole, which is shorter than its diff:
```python
import jax
import jax.numpy as jnp
from jax import lax
from jax.experimental import pallas as pl
from jax.experimental.pallas import tpu as pltpu
from jax.sharding import PartitionSpec as P

EPSILON = 1e-06
GATE_SCALE = 8.0
F32 = jnp.float32
BF16 = jnp.bfloat16
MESH = pl.DeviceIdType.MESH
ROWS = 128
LEN = 512
CH = 512
D = 2048
Q = 512
HID = 1024
SPN = 32


def dot(a, b):
    return jnp.dot(a, b, preferred_element_type=F32)


def iota(shape, dim):
    return lax.broadcasted_iota(jnp.int32, shape, dim)


def one_minus_exp(u):
    series = u * (
        1.0
        - u
        * (
            0.5
            - u
            * (
                1.0 / 6
                - u * (1.0 / 24 - u * (1.0 / 120 - u * (1.0 / 720 - u * (1.0 / 5040))))
            )
        )
    )
    return jnp.where(u < 0.25, series, 1.0 - jnp.exp(-u))


def softplus_neg(d):
    y = jnp.exp(-jnp.abs(d))
    w = 1.0 + y
    near = w - 1.0
    log1p = jnp.where(near == 0.0, y, jnp.log(w) * (y / jnp.where(near == 0.0, 1.0, near)))
    return jnp.maximum(-d, 0.0) + log1p


def shift_of(k):
    c, j = k // 32, k % 32
    dc, dx, dy = j % 2, (j // 2) % 4, (j // 8) % 4
    dz = (c + 8 - dx - dy) % 4
    return dz, dy, dc, dx


def kernel(
    stream,
    cia,
    cib,
    gia,
    gib,
    cwa,
    cwb,
    rga,
    iga,
    rgb,
    igb,
    da,
    db,
    inc,
    owa,
    owb,
    gain,
    ids,
    gp,
    pg,
    wg_hbm,
    wu_hbm,
    wd_hbm,
    out,
    wg,
    wu,
    wd,
    ow,
    xs,
    wb,
    incb,
    a8,
    h8,
    gl,
    hid,
    halo,
    stat,
    carry_in,
    psend,
    rd2,
    prec,
    p0,
    nq,
    mp,
    gm,
    sendb,
    recvb,
    replyb,
    retb,
    xb,
    inner,
    yb,
    acc,
    keys,
    lsem,
    hsem,
    csem,
    psem,
    dsem,
    rsem,
):
    sp = lax.axis_index("sp")
    x = lax.axis_index("tp")
    z, y, core = sp // 8, (sp // 2) % 4, sp % 2

    def device(dz, dy, dc, dx):
        nz, ny, nc = (z + dz) % 4, (y + dy) % 4, (core + dc) % 2
        return {"sp": (nz * 4 + ny) * 2 + nc, "tp": (x + dx) % 4}

    def away(k):
        dz, dy, dc, dx = shift_of(k)
        return device(dz, dy, dc, dx)

    def back(k):
        dz, dy, dc, dx = shift_of(k)
        return device(4 - dz, 4 - dy, 2 - dc, 4 - dx)

    barrier = pltpu.get_barrier_semaphore()

    def greet(k, carry):
        pl.semaphore_signal(barrier, inc=1, device_id=away(k), device_id_type=MESH)
        return carry

    lax.fori_loop(1, 128, greet, 0)

    loads = [
        pltpu.make_async_copy(owa, ow.at[pl.ds(0, 256)], lsem.at[0]),
        pltpu.make_async_copy(owb, ow.at[pl.ds(256, 256)], lsem.at[1]),
        pltpu.make_async_copy(wg_hbm.at[0], wg, lsem.at[2]),
        pltpu.make_async_copy(wu_hbm.at[0], wu, lsem.at[3]),
        pltpu.make_async_copy(wd_hbm.at[0], wd, lsem.at[4]),
    ]
    for load in loads:
        load.start()

    for n, (a_ref, b_ref) in enumerate(((rga, rgb), (iga, igb))):
        for h in range(4):
            place = (iota((64, 256), 1) == iota((64, 256), 0) + 64 * h).astype(BF16)
            wb[n, 64 * h : 64 * h + 64, :] = dot(a_ref[h], place).astype(BF16)
        wb[2 + n] = jnp.zeros((256, 256), BF16)
        for h in range(2):
            wb[2 + n, 128 * h : 128 * h + 128, 128 * h : 128 * h + 128] = b_ref[h]

    for n in range(4):
        row = jnp.broadcast_to(inc[:, 128 * n : 128 * n + 128], (128, 128))
        incb[128 * n : 128 * n + 128, :] = row.T

    xs[0:8, :] = jnp.zeros((8, CH), F32)
    xs[8 : 8 + LEN, 0:256] = cia[...].astype(F32)
    xs[8 : 8 + LEN, 256:512] = cib[...].astype(F32)

    plus = softplus_neg(jnp.concatenate([da[...], db[...]], axis=1)) * GATE_SCALE

    def chunk(step):
        r0 = pl.multiple_of(step * 64, 64)
        jump = incb[pl.ds(r0, 64), :]
        jump = jnp.concatenate([jump, jump], axis=1)
        for side, taps in enumerate((cwa, cwb)):
            lanes = slice(256 * side, 256 * side + 256)
            window = xs[pl.ds(r0, 72), lanes]
            tap = taps[...].astype(F32)
            total = tap[0:1] * pltpu.roll(window, 3, 0)[8:]
            total = total + tap[1:2] * pltpu.roll(window, 2, 0)[8:]
            total = total + tap[2:3] * pltpu.roll(window, 1, 0)[8:]
            total = total + tap[3:4] * window[8:]
            conv = total.astype(BF16)
            rec = jax.nn.sigmoid(dot(conv, wb[2 * side]))
            admit = jax.nn.sigmoid(dot(conv, wb[2 * side + 1]))
            log = jump - rec * plus[:, lanes]
            gone = one_minus_exp(-2.0 * log)
            root = gone * lax.rsqrt(jnp.maximum(gone, 1e-37))
            h = root * admit * conv.astype(F32)
            a = jnp.exp(log)
            a3, h3 = a.reshape(8, 8, 256), h.reshape(8, 8, 256)
            at = iota((8, 8, 256), 1)
            for s in (1, 2, 4):
                ok = at >= s
                ap = jnp.where(ok, pltpu.roll(a3, s, 1), 1.0)
                hp = jnp.where(ok, pltpu.roll(h3, s, 1), 0.0)
                h3 = h3 + a3 * hp
                a3 = a3 * ap
            a8[pl.ds(r0, 64), lanes] = a3.reshape(64, 256)
            h8[pl.ds(r0, 64), lanes] = h3.reshape(64, 256)

    def later_chunks(step, carry):
        chunk(7 - step)
        return carry

    lax.fori_loop(0, 7, later_chunks, 0)

    e0 = jnp.broadcast_to(ids[:, 0:1].astype(F32), (128, 128))
    e1 = jnp.broadcast_to(ids[:, 1:2].astype(F32), (128, 128))
    e0r, e1r = e0.T, e1.T
    earlier = iota((128, 128), 0) < iota((128, 128), 1)
    for n, er in enumerate((e0r, e1r)):
        hits = jnp.where(earlier & (e0 == er), 1.0, 0.0) + jnp.where(earlier & (e1 == er), 1.0, 0.0)
        rank = jnp.sum(hits, axis=0, keepdims=True).astype(jnp.int32)
        e = er[0:1].astype(jnp.int32)
        ez, ey, ec, ex = e // 32, (e // 8) % 4, (e // 4) % 2, e % 4
        dz, dy, dc, dx = (ez - z + 4) % 4, (ey - y + 4) % 4, (ec - core + 2) % 2, (ex - x + 4) % 4
        key = (((dx + dy + dz) % 4) * 32 + dy * 8 + dx * 2 + dc) * 16 + rank
        keys[n] = jnp.broadcast_to(key.astype(F32), (128, 128))
    first = gp[...] * jax.nn.sigmoid(pg[...])
    second = gp[...] * jax.nn.sigmoid(-pg[...])
    keys[2] = jnp.broadcast_to(first, (128, 128)).T
    keys[3] = jnp.broadcast_to(second, (128, 128)).T

    def pack_matrix(step, carry):
        r0 = pl.multiple_of(step * 128, 128)
        rho = (iota((128, 128), 0) + r0).astype(F32)
        k0, k1 = keys[0], keys[1]
        for q in range(4):
            hit = (rho == k0 + 4.0 * q) | (rho == k1 + 4.0 * q)
            mp[pl.ds(r0, 128), 128 * q : 128 * q + 128] = jnp.where(hit, 1.0, 0.0).astype(BF16)
        return carry

    lax.fori_loop(0, 16, pack_matrix, 0)

    pl.semaphore_wait(barrier, 127)
    nextsp = {"sp": (sp + 1) % SPN, "tp": x}
    halos = [
        pltpu.make_async_remote_copy(
            ref.at[pl.ds(LEN - 16, 16)],
            halo.at[n],
            hsem.at[n],
            hsem.at[2 + n],
            device_id=nextsp,
            device_id_type=MESH,
        )
        for n, ref in enumerate((cia, cib))
    ]
    for copy in halos:
        copy.start()

    keys[0] = keys[0].T
    keys[1] = keys[1].T

    def pick_matrix(step, carry):
        r0 = pl.multiple_of(step * 128, 128)
        c, lane = step // 4, step % 4
        rho = (iota((128, 128), 1) + r0).astype(F32)
        k0, k1, w0, w1 = keys[0], keys[1], keys[2], keys[3]
        for q in range(4):
            val = jnp.where(rho == k0 + 4.0 * q, w0, 0.0) + jnp.where(rho == k1 + 4.0 * q, w1, 0.0)
            gm[step, 128 * q : 128 * q + 128, :] = val.astype(BF16)
        return carry

    lax.fori_loop(0, 16, pick_matrix, 0)

    def gelus(step, carry):
        r0 = pl.multiple_of(step * 64, 64)
        gl[pl.ds(r0, 64), 0:256] = jax.nn.gelu(gia[pl.ds(r0, 64), :].astype(F32))
        gl[pl.ds(r0, 64), 256:512] = jax.nn.gelu(gib[pl.ds(r0, 64), :].astype(F32))
        return carry

    lax.fori_loop(0, 8, gelus, 0)

    for copy in halos:
        copy.wait()
    keep = jnp.where(sp > 0, 1.0, 0.0)
    xs[0:8, 0:256] = halo[0].astype(F32)[8:16] * keep
    xs[0:8, 256:512] = halo[1].astype(F32)[8:16] * keep
    chunk(0)

    def link(step, carry):
        prod, state = carry
        for n in range(8):
            r0 = pl.multiple_of(step * 64, 64) + 8 * n
            a, h = a8[pl.ds(r0, 8), :], h8[pl.ds(r0, 8), :]
            h = h + a * state
            a = a * prod
            a8[pl.ds(r0, 8), :] = a
            h8[pl.ds(r0, 8), :] = h
            prod, state = a[7:8], h[7:8]
        return prod, state

    prod, state = lax.fori_loop(0, 8, link, (jnp.ones((1, CH), F32), jnp.zeros((1, CH), F32)))
    for n in range(4):
        stat[n : n + 1, :] = prod[:, 128 * n : 128 * n + 128]
        stat[4 + n : 5 + n, :] = state[:, 128 * n : 128 * n + 128]

    def tell(k, carry):
        pltpu.make_async_remote_copy(
            stat,
            carry_in.at[k],
            csem.at[0],
            csem.at[1],
            device_id={"sp": (sp + k) % SPN, "tp": x},
            device_id_type=MESH,
        ).start()
        return carry

    lax.fori_loop(1, SPN, tell, 0)
    told = carry_in.at[pl.ds(1, SPN - 1)]
    pltpu.make_async_copy(told, told, csem.at[1]).wait()

    enter = jnp.zeros((4, 128), F32)
    for k in range(SPN - 1, 0, -1):
        enter = jnp.where(k <= sp, carry_in[k, 0:4] * enter + carry_in[k, 4:8], enter)
    enter = jnp.concatenate([enter[n : n + 1] for n in range(4)], axis=1)

    def hiddens(step, carry):
        r0 = pl.multiple_of(step * 64, 64)
        states = h8[pl.ds(r0, 64), :] + a8[pl.ds(r0, 64), :] * enter
        hid[pl.ds(r0, 64), :] = (states * gl[pl.ds(r0, 64), :]).astype(BF16)
        return carry

    lax.fori_loop(0, 8, hiddens, 0)

    loads[0].wait()
    loads[1].wait()

    def rows_for(d):
        return hid[pl.ds(pl.multiple_of(((x + d) % 4) * 128, 128), 128), :]

    def project(d, half, extra=None):
        rows = rows_for(d)
        for n in range(2):
            at = 1024 * half + 512 * n
            part = dot(rows, ow[:, at : at + 512])
            if extra is not None:
                part = part + extra[:, 512 * n : 512 * n + 512].astype(F32)
            psend[2 * d + half - 2, :, 512 * n : 512 * n + 512] = part.astype(BF16)

    def push(d, half, dst, sem, dx):
        copy = pltpu.make_async_remote_copy(
            psend.at[2 * d + half - 2],
            dst,
            psem.at[2 * sem],
            psem.at[2 * sem + 1],
            device_id={"sp": sp, "tp": (x + dx) % 4},
            device_id_type=MESH,
        )
        copy.start()
        return copy

    project(2, 0)
    sums = [push(2, 0, rd2.at[0], 0, 1)]
    project(2, 1)
    sums.append(push(2, 1, rd2.at[1], 1, 3))
    project(1, 1)
    sums.append(push(1, 1, prec.at[1], 2, 1))
    project(3, 0)
    sums.append(push(3, 0, prec.at[2], 3, 3))
    own = rows_for(0)
    for n in range(4):
        p0[:, 512 * n : 512 * n + 512] = dot(own, ow[:, 512 * n : 512 * n + 512])
    sums[0].wait_recv()
    project(1, 0, rd2.at[0])
    sums.append(push(1, 0, prec.at[0], 4, 1))
    sums[1].wait_recv()
    project(3, 1, rd2.at[1])
    sums.append(push(3, 1, prec.at[3], 5, 3))
    for copy in sums[2:]:
        copy.wait_recv()

    gains = gain[...].astype(F32)

    def norms(step, carry):
        r0 = pl.multiple_of(step * 16, 16)
        rows = pl.ds(r0, 16)
        mixed = p0[rows, :]
        left = jnp.concatenate([prec[0, rows, :], prec[1, rows, :]], axis=1).astype(F32)
        right = jnp.concatenate([prec[2, rows, :], prec[3, rows, :]], axis=1).astype(F32)
        middle = (stream[rows, :].astype(F32) + (mixed + left + right)).astype(BF16).astype(F32)
        scale = lax.rsqrt(jnp.mean(middle * middle, axis=-1, keepdims=True) + EPSILON)
        normed = (middle * scale * gains).astype(BF16)
        for q in range(4):
            acc[pl.ds(128 * q + r0, 16), :] = middle[:, 512 * q : 512 * q + 512]
            nq[pl.ds(128 * q + r0, 16), :] = normed[:, 512 * q : 512 * q + 512]
        return carry

    lax.fori_loop(0, 8, norms, 0)

    def tile(k):
        return pl.ds(pl.multiple_of(k * 16, 16), 16)

    def out_copy(k):
        return pltpu.make_async_remote_copy(
            sendb.at[tile(k)],
            recvb.at[tile(k)],
            dsem.at[0],
            dsem.at[1 + k // 32],
            device_id=away(k),
            device_id_type=MESH,
        )

    def home_copy(k):
        return pltpu.make_async_remote_copy(
            replyb.at[tile(k)],
            retb.at[tile(k)],
            rsem.at[0],
            rsem.at[1 + k // 32],
            device_id=back(k),
            device_id_type=MESH,
        )

    def dispatch(c, carry):
        for n in range(4):
            r0 = pl.multiple_of(c * 512, 512) + 128 * n
            sendb[pl.ds(r0, 128), :] = dot(mp[pl.ds(r0, 128), :], nq[...]).astype(BF16)

        def go(k, inside):
            out_copy(k).start()
            return inside

        lax.fori_loop(jnp.maximum(c * 32, 1), c * 32 + 32, go, 0)
        return carry

    lax.fori_loop(0, 4, dispatch, 0)
    recvb[0:16, :] = sendb[0:16, :]

    loads[2].wait()
    loads[3].wait()
    loads[4].wait()

    def wait_class(buf, sem, c):
        @pl.when(c == 0)
        def _():
            part = buf.at[pl.ds(16, 496)]
            pltpu.make_async_copy(part, part, sem.at[1]).wait()

        @pl.when(c > 0)
        def _():
            part = buf.at[pl.ds(pl.multiple_of(c * 512, 512), 512)]
            pltpu.make_async_copy(part, part, sem.at[1 + c]).wait()

    def experts(c, carry):
        wait_class(recvb, dsem, c)
        ra, rb = iota((256, 256), 0), iota((256, 256), 1)
        sort = (rb == ((ra % 64) // 4) * 16 + (ra // 64) * 4 + ra % 4).astype(F32).astype(BF16)
        unsort = (ra == ((rb % 64) // 4) * 16 + (rb // 64) * 4 + rb % 4).astype(F32).astype(BF16)
        for half in range(2):
            r0 = pl.multiple_of(c * 512, 512) + 256 * half
            got = dot(sort, recvb[pl.ds(r0, 256), :]).astype(BF16)
            for q in range(4):
                xb[64 * half : 64 * half + 64, 512 * q : 512 * q + 512] = got[64 * q : 64 * q + 64]
        for n in range(4):
            cols = slice(256 * n, 256 * n + 256)
            gate = dot(xb[...], wg[:, cols])
            up = dot(xb[...], wu[:, cols])
            inner[:, cols] = (jax.nn.silu(gate) * up).astype(BF16)
        for q in range(4):
            down = dot(inner[...], wd[:, 512 * q : 512 * q + 512]).astype(BF16)
            for half in range(2):
                yb[half, 64 * q : 64 * q + 64, :] = down[64 * half : 64 * half + 64]
        for half in range(2):
            r0 = pl.multiple_of(c * 512, 512) + 256 * half
            replyb[pl.ds(r0, 256), :] = dot(unsort, yb[half]).astype(BF16)

        def go(k, inside):
            home_copy(k).start()
            return inside

        lax.fori_loop(jnp.maximum(c * 32, 1), c * 32 + 32, go, 0)
        return carry

    lax.fori_loop(0, 4, experts, 0)
    retb[0:16, :] = replyb[0:16, :]

    def combine(c, carry):
        wait_class(retb, rsem, c)
        for n in range(4):
            rows = slice(128 * n, 128 * n + 128)
            part = acc[rows, :]
            for lane in range(4):
                r0 = pl.multiple_of(c * 512, 512) + 128 * lane
                part = part + dot(gm[4 * c + lane, rows, :], retb[pl.ds(r0, 128), :])
            acc[rows, :] = part
        return carry

    lax.fori_loop(0, 4, combine, 0)
    for q in range(4):
        out[:, 512 * q : 512 * q + 512] = acc[128 * q : 128 * q + 128, :].astype(BF16)

    pltpu.make_async_copy(told, told, csem.at[0]).wait()
    for copy in sums:
        copy.wait_send()
    for buf, sem in ((sendb, dsem), (replyb, rsem)):
        part = buf.at[pl.ds(16, 2032)]
        pltpu.make_async_copy(part, part, sem.at[0]).wait()


def shards(*args):
    (
        stream,
        cia,
        cib,
        gia,
        gib,
        cwa,
        cwb,
        rga,
        iga,
        rgb,
        igb,
        da,
        db,
        inc,
        owa,
        owb,
        gain,
        ids,
        gp,
        pg,
        wg,
        wu,
        wd,
    ) = args
    row = lambda a: a.reshape(1, -1)
    operands = (
        stream,
        cia,
        cib,
        gia,
        gib,
        cwa,
        cwb,
        rga,
        iga,
        rgb,
        igb,
        row(da),
        row(db),
        row(inc),
        owa,
        owb,
        row(gain),
        ids,
        row(gp),
        row(pg),
        wg,
        wu,
        wd,
    )
    vmem = pl.BlockSpec(memory_space=pltpu.VMEM)
    far = pl.BlockSpec(memory_space=pl.ANY)
    specs = [vmem] * len(operands)
    for n in (14, 15, 20, 21, 22):
        specs[n] = far
    V = pltpu.VMEM
    return pl.pallas_call(
        kernel,
        out_shape=jax.ShapeDtypeStruct((ROWS, D), BF16),
        in_specs=specs,
        out_specs=vmem,
        scratch_shapes=[
            V((D, HID), BF16),
            V((D, HID), BF16),
            V((HID, D), BF16),
            V((CH, D), BF16),
            V((LEN + 8, CH), F32),
            V((4, 256, 256), BF16),
            V((LEN, 128), F32),
            V((LEN, CH), F32),
            V((LEN, CH), F32),
            V((LEN, CH), F32),
            V((LEN, CH), BF16),
            V((2, 16, 256), BF16),
            V((8, 128), F32),
            V((SPN, 8, 128), F32),
            V((6, ROWS, 1024), BF16),
            V((2, ROWS, 1024), BF16),
            V((4, ROWS, 1024), BF16),
            V((ROWS, D), F32),
            V((512, Q), BF16),
            V((2048, 512), BF16),
            V((16, 512, 128), BF16),
            V((2048, Q), BF16),
            V((2048, Q), BF16),
            V((2048, Q), BF16),
            V((2048, Q), BF16),
            V((128, D), BF16),
            V((128, HID), BF16),
            V((2, 256, Q), BF16),
            V((512, Q), F32),
            V((4, 128, 128), F32),
            pltpu.SemaphoreType.DMA((5,)),
            pltpu.SemaphoreType.DMA((4,)),
            pltpu.SemaphoreType.DMA((2,)),
            pltpu.SemaphoreType.DMA((12,)),
            pltpu.SemaphoreType.DMA((5,)),
            pltpu.SemaphoreType.DMA((5,)),
        ],
        compiler_params=pltpu.CompilerParams(
            collective_id=0, has_side_effects=True, vmem_limit_bytes=58 * 1024 * 1024
        ),
        name="layer",
    )(*operands)


def solution(mesh):
    placed = (
        P(("sp", "tp"), None),
        P("sp", "tp"),
        P("sp", "tp"),
        P("sp", "tp"),
        P("sp", "tp"),
        P(None, "tp"),
        P(None, "tp"),
        P("tp", None, None),
        P("tp", None, None),
        P("tp", None, None),
        P("tp", None, None),
        P("tp"),
        P("tp"),
        P("sp"),
        P("tp", None),
        P("tp", None),
        P(),
        P(("sp", "tp"), None),
        P(("sp", "tp")),
        P(("sp", "tp")),
        P(("sp", "tp"), None, None),
        P(("sp", "tp"), None, None),
        P(("sp", "tp"), None, None),
    )
    return jax.shard_map(
        shards, mesh=mesh, in_specs=placed, out_specs=P(("sp", "tp"), None), check_vma=False
    )
```

time: 242 us -> 110 us (0.45)
  the two profiles are of different devices: /device:TPU:1 before, /device:TPU:3 now
where the time goes in v1:
time: 110 us
  Pallas kernels  105 us (95%)
  local copies, waits for them, and re-layouts  4.58 us (4%)
    pallas_call x1, Pallas kernels, shards(): pl.pallas_call(kernel, out_shape=jax.ShapeDtypeStruct((ROWS, D), BF16), i...  105 us
    unnamed x2, local copies, waits for them, and re-layouts  3.29 us

profile of v1, /device:TPU:3, one launch (start us, length us, event | category | flops | bytes accessed | tf_op | source)
XLA Modules:
  0.0 109.7 jit_solution(9359388311459433958)
XLA Ops:
  0.0 1.3 %reshape.21.gain = bf16[1,2048]{1,0:T(2,128)(2,1)} reshape(bf16[2048]{0:T(1024)(128)(2,1)} %param.39) | data formatting | bytes 8192 | tf_op jit(solution)/shard_map/reshape | solution.py:531
  1.3 1.4 %copy.24.ids = s32[128,2]{1,0:T(8,128)} copy(s32[128,2]{0,1:T(2,128)} %param.40) | data formatting | bytes 2048 | tf_op args[17]
  2.7 105.1 %layer.1 = bf16[128,2048]{1,0:T(8,128)(2,1)} custom-call(bf16[128,2048]{1,0:T(8,128)(2,1)} %stream.1, bf16[512,256]{1,0:T(8,128)(2,1)} %cia.1, bf16[512,256]{1,0:T(8,128)(2,1)} %cib.1, bf16[512,256]{1,0:T(8,128)(2,1)} %gia.1, bf16[512,256]{1,0:T(8,128)(2,1)} %gib.1, bf16[4,256]{1,0:T(4,128)(2,1)} %cwa.1, bf16[4,256]{1,0:T(4,128)(2,1)} %cwb.1, ...), custom_call_target="tpu_custom_call" | custom-call | tf_op jit(solution)/shard_map/layer/pallas_call | solution.py:563
  107.8 1.9 %copy.26 = bf16[128,2048]{1,0:T(8,128)(2,1)} copy(bf16[128,2048]{1,0:T(8,128)(2,1)} %layer.1) | data formatting | bytes 1048576

commit v2 on v1

--- a/solution.py
+++ b/solution.py
@@ -51,14 +51,31 @@
     return jnp.maximum(-d, 0.0) + log1p
 
 
-def shift_of(k):
-    c, j = k // 32, k % 32
-    dc, dx, dy = j % 2, (j // 2) % 4, (j // 8) % 4
-    dz = (c + 8 - dx - dy) % 4
-    return dz, dy, dc, dx
-
-
 def kernel(
+    stream_far,
+    cia_far,
+    cib_far,
+    gia_far,
+    gib_far,
+    cwa_far,
+    cwb_far,
+    rga_far,
+    iga_far,
+    rgb_far,
+    igb_far,
+    da_far,
+    db_far,
+    inc_far,
+    owa_far,
+    owb_far,
+    gain_far,
+    ids_far,
+    gp_far,
+    pg_far,
+    wg_far,
+    wu_far,
+    wd_far,
+    out,
     stream,
     cia,
     cib,
@@ -73,16 +90,10 @@
     da,
     db,
     inc,
-    owa,
-    owb,
     gain,
     ids,
     gp,
     pg,
-    wg_hbm,
-    wu_hbm,
-    wd_hbm,
-    out,
     wg,
     wu,
     wd,
@@ -124,35 +135,67 @@
     x = lax.axis_index("tp")
     z, y, core = sp // 8, (sp // 2) % 4, sp % 2
 
-    def device(dz, dy, dc, dx):
-        nz, ny, nc = (z + dz) % 4, (y + dy) % 4, (core + dc) % 2
-        return {"sp": (nz * 4 + ny) * 2 + nc, "tp": (x + dx) % 4}
-
-    def away(k):
-        dz, dy, dc, dx = shift_of(k)
-        return device(dz, dy, dc, dx)
-
-    def back(k):
-        dz, dy, dc, dx = shift_of(k)
-        return device(4 - dz, 4 - dy, 2 - dc, 4 - dx)
+    xs_at = [lax.rem(x + n, 4) for n in range(4)]
+    ys_at = [lax.rem(y + n, 4) * 2 for n in range(4)]
+    zs_at = [lax.rem(z + n, 4) * 8 for n in range(4)]
+    cores_at = [core, 1 - core]
+    yc_at = [[ys_at[n] + cores_at[m] for m in range(2)] for n in range(4)]
+
+    def class_devices(c, sign):
+        zc = [lax.rem(z + sign * (c - n) + 16, 4) * 8 for n in range(7)]
+        found = []
+        for j in range(32):
+            dc, dx, dy = j % 2, (j // 2) % 4, j // 8
+            spot = zc[dx + dy] + yc_at[(sign * dy) % 4][dc]
+            found.append({"sp": spot, "tp": xs_at[(sign * dx) % 4]})
+        return found
+
+    pairs = (
+        (cia_far, cia),
+        (cib_far, cib),
+        (cwa_far, cwa),
+        (cwb_far, cwb),
+        (rga_far, rga),
+        (iga_far, iga),
+        (rgb_far, rgb),
+        (igb_far, igb),
+        (da_far, da),
+        (db_far, db),
+        (inc_far, inc),
+        (ids_far, ids),
+        (gp_far, gp),
+        (pg_far, pg),
+        (gia_far, gia),
+        (gib_far, gib),
+        (owa_far, ow.at[pl.ds(0, 256)]),
+        (owb_far, ow.at[pl.ds(256, 256)]),
+        (stream_far, stream),
+        (gain_far, gain),
+        (wg_far.at[0], wg),
+        (wu_far.at[0], wu),
+        (wd_far.at[0], wd),
+    )
+    copies = [pltpu.make_async_copy(src, dst, lsem.at[n]) for n, (src, dst) in enumerate(pairs)]
+    for copy in copies:
+        copy.start()
+    early, middle_loads, loads = copies[:14], copies[14:16], copies[16:]
 
     barrier = pltpu.get_barrier_semaphore()
-
-    def greet(k, carry):
-        pl.semaphore_signal(barrier, inc=1, device_id=away(k), device_id_type=MESH)
-        return carry
-
-    lax.fori_loop(1, 128, greet, 0)
-
-    loads = [
-        pltpu.make_async_copy(owa, ow.at[pl.ds(0, 256)], lsem.at[0]),
-        pltpu.make_async_copy(owb, ow.at[pl.ds(256, 256)], lsem.at[1]),
-        pltpu.make_async_copy(wg_hbm.at[0], wg, lsem.at[2]),
-        pltpu.make_async_copy(wu_hbm.at[0], wu, lsem.at[3]),
-        pltpu.make_async_copy(wd_hbm.at[0], wd, lsem.at[4]),
-    ]
-    for load in loads:
-        load.start()
+    for dz in range(4):
+        for dy in range(4):
+            for dc in range(2):
+                spot = zs_at[dz] + yc_at[dy][dc]
+                for dx in range(4):
+                    if dz or dy or dc or dx:
+                        pl.semaphore_signal(
+                            barrier,
+                            inc=1,
+                            device_id={"sp": spot, "tp": xs_at[dx]},
+                            device_id_type=MESH,
+                        )
+
+    for load in early:
+        load.wait()
 
     for n, (a_ref, b_ref) in enumerate(((rga, rgb), (iga, igb))):
         for h in range(4):
@@ -209,9 +252,9 @@
 
     lax.fori_loop(0, 7, later_chunks, 0)
 
-    e0 = jnp.broadcast_to(ids[:, 0:1].astype(F32), (128, 128))
-    e1 = jnp.broadcast_to(ids[:, 1:2].astype(F32), (128, 128))
-    e0r, e1r = e0.T, e1.T
+    e0r = jnp.broadcast_to(ids[0:1, :].astype(F32), (128, 128))
+    e1r = jnp.broadcast_to(ids[1:2, :].astype(F32), (128, 128))
+    e0, e1 = e0r.T, e1r.T
     earlier = iota((128, 128), 0) < iota((128, 128), 1)
     for n, er in enumerate((e0r, e1r)):
         hits = jnp.where(earlier & (e0 == er), 1.0, 0.0) + jnp.where(earlier & (e1 == er), 1.0, 0.0)
@@ -268,6 +311,9 @@
 
     lax.fori_loop(0, 16, pick_matrix, 0)
 
+    for load in middle_loads:
+        load.wait()
+
     def gelus(step, carry):
         r0 = pl.multiple_of(step * 64, 64)
         gl[pl.ds(r0, 64), 0:256] = jax.nn.gelu(gia[pl.ds(r0, 64), :].astype(F32))
@@ -300,18 +346,15 @@
         stat[n : n + 1, :] = prod[:, 128 * n : 128 * n + 128]
         stat[4 + n : 5 + n, :] = state[:, 128 * n : 128 * n + 128]
 
-    def tell(k, carry):
+    for k in range(1, SPN):
         pltpu.make_async_remote_copy(
             stat,
             carry_in.at[k],
             csem.at[0],
             csem.at[1],
-            device_id={"sp": (sp + k) % SPN, "tp": x},
+            device_id={"sp": lax.rem(sp + k, SPN), "tp": x},
             device_id_type=MESH,
         ).start()
-        return carry
-
-    lax.fori_loop(1, SPN, tell, 0)
     told = carry_in.at[pl.ds(1, SPN - 1)]
     pltpu.make_async_copy(told, told, csem.at[1]).wait()
 
@@ -375,7 +418,10 @@
     for copy in sums[2:]:
         copy.wait_recv()
 
+    loads[2].wait()
+    loads[3].wait()
     gains = gain[...].astype(F32)
+    gains = jnp.concatenate([gains[n : n + 1] for n in range(16)], axis=1)
 
     def norms(step, carry):
         r0 = pl.multiple_of(step * 16, 16)
@@ -393,47 +439,35 @@
 
     lax.fori_loop(0, 8, norms, 0)
 
-    def tile(k):
-        return pl.ds(pl.multiple_of(k * 16, 16), 16)
-
-    def out_copy(k):
-        return pltpu.make_async_remote_copy(
-            sendb.at[tile(k)],
-            recvb.at[tile(k)],
-            dsem.at[0],
-            dsem.at[1 + k // 32],
-            device_id=away(k),
-            device_id_type=MESH,
-        )
-
-    def home_copy(k):
-        return pltpu.make_async_remote_copy(
-            replyb.at[tile(k)],
-            retb.at[tile(k)],
-            rsem.at[0],
-            rsem.at[1 + k // 32],
-            device_id=back(k),
-            device_id_type=MESH,
-        )
+    def send_class(c, src, dst, sem, sign):
+        for j, peer in enumerate(class_devices(c, sign)):
+            tile = pl.ds(pl.multiple_of(c * 512, 512) + 16 * j, 16)
+            copy = pltpu.make_async_remote_copy(
+                src.at[tile],
+                dst.at[tile],
+                sem.at[0],
+                sem.at[1 + c],
+                device_id=peer,
+                device_id_type=MESH,
+            )
+            if j == 0:
+                pl.when(c > 0)(copy.start)
+            else:
+                copy.start()
 
     def dispatch(c, carry):
         for n in range(4):
             r0 = pl.multiple_of(c * 512, 512) + 128 * n
             sendb[pl.ds(r0, 128), :] = dot(mp[pl.ds(r0, 128), :], nq[...]).astype(BF16)
 
-        def go(k, inside):
-            out_copy(k).start()
-            return inside
-
-        lax.fori_loop(jnp.maximum(c * 32, 1), c * 32 + 32, go, 0)
+        send_class(c, sendb, recvb, dsem, 1)
         return carry
 
     lax.fori_loop(0, 4, dispatch, 0)
     recvb[0:16, :] = sendb[0:16, :]
 
-    loads[2].wait()
-    loads[3].wait()
-    loads[4].wait()
+    for load in loads[4:]:
+        load.wait()
 
     def wait_class(buf, sem, c):
         @pl.when(c == 0)
@@ -469,11 +503,7 @@
             r0 = pl.multiple_of(c * 512, 512) + 256 * half
             replyb[pl.ds(r0, 256), :] = dot(unsort, yb[half]).astype(BF16)
 
-        def go(k, inside):
-            home_copy(k).start()
-            return inside
-
-        lax.fori_loop(jnp.maximum(c * 32, 1), c * 32 + 32, go, 0)
+        send_class(c, replyb, retb, rsem, -1)
         return carry
 
     lax.fori_loop(0, 4, experts, 0)
@@ -546,8 +576,8 @@
         row(inc),
         owa,
         owb,
-        row(gain),
-        ids,
+        gain.reshape(16, 128),
+        ids.T,
         row(gp),
         row(pg),
         wg,
@@ -556,16 +586,15 @@
     )
     vmem = pl.BlockSpec(memory_space=pltpu.VMEM)
     far = pl.BlockSpec(memory_space=pl.ANY)
-    specs = [vmem] * len(operands)
-    for n in (14, 15, 20, 21, 22):
-        specs[n] = far
     V = pltpu.VMEM
+    near = [V(a.shape, a.dtype) for n, a in enumerate(operands[:20]) if n not in (14, 15)]
     return pl.pallas_call(
         kernel,
-        out_shape=jax.ShapeDtypeStruct((ROWS, D), BF16),
-        in_specs=specs,
+        out_shape=pltpu.VMEM((ROWS, D), BF16),
+        in_specs=[far] * len(operands),
         out_specs=vmem,
-        scratch_shapes=[
+        scratch_shapes=near
+        + [
             V((D, HID), BF16),
             V((D, HID), BF16),
             V((HID, D), BF16),
@@ -596,7 +625,7 @@
             V((2, 256, Q), BF16),
             V((512, Q), F32),
             V((4, 128, 128), F32),
-            pltpu.SemaphoreType.DMA((5,)),
+            pltpu.SemaphoreType.DMA((23,)),
             pltpu.SemaphoreType.DMA((4,)),
             pltpu.SemaphoreType.DMA((2,)),
             pltpu.SemaphoreType.DMA((12,)),

time: 110 us -> 96.1 us (0.87)
  the two profiles are of different devices: /device:TPU:3 before, /device:TPU:33 now
where the time goes in v2:
time: 96.1 us; the launch traced here: 96 us
  Pallas kernels  95.1 us (99%)
    pallas_call x1, Pallas kernels, shards(): pl.pallas_call(kernel, out_shape=pltpu.VMEM((ROWS, D), BF16), in_specs=[f...  95.1 us

profile of v2, /device:TPU:33, one launch (start us, length us, event | category | flops | bytes accessed | tf_op | source)
XLA Modules:
  0.0 96.0 jit_solution(17392886631256077407)
XLA Ops:
  0.0 95.1 %layer.1 = bf16[128,2048]{1,0:T(8,128)(2,1)S(1)} custom-call(bf16[128,2048]{1,0:T(8,128)(2,1)} %stream_far.1, bf16[512,256]{1,0:T(8,128)(2,1)} %cia_far.1, bf16[512,256]{1,0:T(8,128)(2,1)} %cib_far.1, bf16[512,256]{1,0:T(8,128)(2,1)} %gia_far.1, bf16[512,256]{1,0:T(8,128)(2,1)} %gib_far.1, bf16[4,256]{1,0:T(4,128)(2,1)} %cwa_far.1, bf16[4,256]{1,0:T(4,128)(2,1)} %cwb_far.1, ...), custom_call_target="tpu_custom_call" | custom-call | tf_op jit(solution)/shard_map/layer/pallas_call | solution.py:591
  95.2 0.8 copy.25

commit v3 on v2

--- a/solution.py
+++ b/solution.py
@@ -27,20 +27,10 @@
     return lax.broadcasted_iota(jnp.int32, shape, dim)
 
 
-def one_minus_exp(u):
-    series = u * (
-        1.0
-        - u
-        * (
-            0.5
-            - u
-            * (
-                1.0 / 6
-                - u * (1.0 / 24 - u * (1.0 / 120 - u * (1.0 / 720 - u * (1.0 / 5040))))
-            )
-        )
-    )
-    return jnp.where(u < 0.25, series, 1.0 - jnp.exp(-u))
+def one_minus_square(log, a):
+    u = -2.0 * log
+    series = u * (1.0 - u * (0.5 - u * (1.0 / 6 - u * (1.0 / 24 - u * (1.0 / 120)))))
+    return jnp.where(u < 0.05, series, 1.0 - a * a)
 
 
 def softplus_neg(d):
@@ -229,12 +219,12 @@
             total = total + tap[3:4] * window[8:]
             conv = total.astype(BF16)
             rec = jax.nn.sigmoid(dot(conv, wb[2 * side]))
-            admit = jax.nn.sigmoid(dot(conv, wb[2 * side + 1]))
+            admit = 0.5 * jnp.tanh(0.5 * dot(conv, wb[2 * side + 1])) + 0.5
             log = jump - rec * plus[:, lanes]
-            gone = one_minus_exp(-2.0 * log)
+            a = jnp.exp(log)
+            gone = one_minus_square(log, a)
             root = gone * lax.rsqrt(jnp.maximum(gone, 1e-37))
             h = root * admit * conv.astype(F32)
-            a = jnp.exp(log)
             a3, h3 = a.reshape(8, 8, 256), h.reshape(8, 8, 256)
             at = iota((8, 8, 256), 1)
             for s in (1, 2, 4):
@@ -250,7 +240,59 @@
         chunk(7 - step)
         return carry
 
-    lax.fori_loop(0, 7, later_chunks, 0)
+    lax.fori_loop(0, 4, later_chunks, 0)
+    pl.semaphore_wait(barrier, 127)
+    nextsp = {"sp": (sp + 1) % SPN, "tp": x}
+    halos = [
+        pltpu.make_async_remote_copy(
+            ref.at[pl.ds(LEN - 16, 16)],
+            halo.at[n],
+            hsem.at[n],
+            hsem.at[2 + n],
+            device_id=nextsp,
+            device_id_type=MESH,
+        )
+        for n, ref in enumerate((cia, cib))
+    ]
+    for copy in halos:
+        copy.start()
+
+    lax.fori_loop(4, 7, later_chunks, 0)
+
+    for copy in halos:
+        copy.wait()
+    keep = jnp.where(sp > 0, 1.0, 0.0)
+    xs[0:8, 0:256] = halo[0].astype(F32)[8:16] * keep
+    xs[0:8, 256:512] = halo[1].astype(F32)[8:16] * keep
+    chunk(0)
+
+    def link(step, carry):
+        prod, state = carry
+        for n in range(8):
+            r0 = pl.multiple_of(step * 64, 64) + 8 * n
+            a, h = a8[pl.ds(r0, 8), :], h8[pl.ds(r0, 8), :]
+            h = h + a * state
+            a = a * prod
+            a8[pl.ds(r0, 8), :] = a
+            h8[pl.ds(r0, 8), :] = h
+            prod, state = a[7:8], h[7:8]
+        return prod, state
+
+    prod, state = lax.fori_loop(0, 8, link, (jnp.ones((1, CH), F32), jnp.zeros((1, CH), F32)))
+    for n in range(4):
+        stat[n : n + 1, :] = prod[:, 128 * n : 128 * n + 128]
+        stat[4 + n : 5 + n, :] = state[:, 128 * n : 128 * n + 128]
+
+    for k in range(1, SPN):
+        pltpu.make_async_remote_copy(
+            stat,
+            carry_in.at[k],
+            csem.at[0],
+            csem.at[1],
+            device_id={"sp": lax.rem(sp + k, SPN), "tp": x},
+            device_id_type=MESH,
+        ).start()
+    told = carry_in.at[pl.ds(1, SPN - 1)]
 
     e0r = jnp.broadcast_to(ids[0:1, :].astype(F32), (128, 128))
     e1r = jnp.broadcast_to(ids[1:2, :].astype(F32), (128, 128))
@@ -280,22 +322,6 @@
 
     lax.fori_loop(0, 16, pack_matrix, 0)
 
-    pl.semaphore_wait(barrier, 127)
-    nextsp = {"sp": (sp + 1) % SPN, "tp": x}
-    halos = [
-        pltpu.make_async_remote_copy(
-            ref.at[pl.ds(LEN - 16, 16)],
-            halo.at[n],
-            hsem.at[n],
-            hsem.at[2 + n],
-            device_id=nextsp,
-            device_id_type=MESH,
-        )
-        for n, ref in enumerate((cia, cib))
-    ]
-    for copy in halos:
-        copy.start()
-
     keys[0] = keys[0].T
     keys[1] = keys[1].T
 
@@ -322,40 +348,6 @@
 
     lax.fori_loop(0, 8, gelus, 0)
 
-    for copy in halos:
-        copy.wait()
-    keep = jnp.where(sp > 0, 1.0, 0.0)
-    xs[0:8, 0:256] = halo[0].astype(F32)[8:16] * keep
-    xs[0:8, 256:512] = halo[1].astype(F32)[8:16] * keep
-    chunk(0)
-
-    def link(step, carry):
-        prod, state = carry
-        for n in range(8):
-            r0 = pl.multiple_of(step * 64, 64) + 8 * n
-            a, h = a8[pl.ds(r0, 8), :], h8[pl.ds(r0, 8), :]
-            h = h + a * state
-            a = a * prod
-            a8[pl.ds(r0, 8), :] = a
-            h8[pl.ds(r0, 8), :] = h
-            prod, state = a[7:8], h[7:8]
-        return prod, state
-
-    prod, state = lax.fori_loop(0, 8, link, (jnp.ones((1, CH), F32), jnp.zeros((1, CH), F32)))
-    for n in range(4):
-        stat[n : n + 1, :] = prod[:, 128 * n : 128 * n + 128]
-        stat[4 + n : 5 + n, :] = state[:, 128 * n : 128 * n + 128]
-
-    for k in range(1, SPN):
-        pltpu.make_async_remote_copy(
-            stat,
-            carry_in.at[k],
-            csem.at[0],
-            csem.at[1],
-            device_id={"sp": lax.rem(sp + k, SPN), "tp": x},
-            device_id_type=MESH,
-        ).start()
-    told = carry_in.at[pl.ds(1, SPN - 1)]
     pltpu.make_async_copy(told, told, csem.at[1]).wait()
 
     enter = jnp.zeros((4, 128), F32)
@@ -364,15 +356,14 @@
     enter = jnp.concatenate([enter[n : n + 1] for n in range(4)], axis=1)
 
     def hiddens(step, carry):
-        r0 = pl.multiple_of(step * 64, 64)
+        r0 = pl.multiple_of(lax.rem(step + 2 * x + 4, 8) * 64, 64)
         states = h8[pl.ds(r0, 64), :] + a8[pl.ds(r0, 64), :] * enter
         hid[pl.ds(r0, 64), :] = (states * gl[pl.ds(r0, 64), :]).astype(BF16)
         return carry
 
-    lax.fori_loop(0, 8, hiddens, 0)
-
     loads[0].wait()
     loads[1].wait()
+    lax.fori_loop(0, 2, hiddens, 0)
 
     def rows_for(d):
         return hid[pl.ds(pl.multiple_of(((x + d) % 4) * 128, 128), 128), :]
@@ -402,6 +393,7 @@
     sums = [push(2, 0, rd2.at[0], 0, 1)]
     project(2, 1)
     sums.append(push(2, 1, rd2.at[1], 1, 3))
+    lax.fori_loop(2, 8, hiddens, 0)
     project(1, 1)
     sums.append(push(1, 1, prec.at[1], 2, 1))
     project(3, 0)
@@ -415,21 +407,28 @@
     sums[1].wait_recv()
     project(3, 1, rd2.at[1])
     sums.append(push(3, 1, prec.at[3], 5, 3))
-    for copy in sums[2:]:
-        copy.wait_recv()
-
     loads[2].wait()
     loads[3].wait()
+    for copy in sums[2:4]:
+        copy.wait_recv()
+
+    def gather(step, carry):
+        rows = pl.ds(pl.multiple_of(step * 16, 16), 16)
+        part = jnp.concatenate([prec[2, rows, :], prec[1, rows, :]], axis=1).astype(F32)
+        p0[rows, :] = p0[rows, :] + part + stream[rows, :].astype(F32)
+        return carry
+
+    lax.fori_loop(0, 8, gather, 0)
+    for copy in sums[4:]:
+        copy.wait_recv()
     gains = gain[...].astype(F32)
     gains = jnp.concatenate([gains[n : n + 1] for n in range(16)], axis=1)
 
     def norms(step, carry):
         r0 = pl.multiple_of(step * 16, 16)
         rows = pl.ds(r0, 16)
-        mixed = p0[rows, :]
-        left = jnp.concatenate([prec[0, rows, :], prec[1, rows, :]], axis=1).astype(F32)
-        right = jnp.concatenate([prec[2, rows, :], prec[3, rows, :]], axis=1).astype(F32)
-        middle = (stream[rows, :].astype(F32) + (mixed + left + right)).astype(BF16).astype(F32)
+        part = jnp.concatenate([prec[0, rows, :], prec[3, rows, :]], axis=1).astype(F32)
+        middle = (p0[rows, :] + part).astype(BF16).astype(F32)
         scale = lax.rsqrt(jnp.mean(middle * middle, axis=-1, keepdims=True) + EPSILON)
         normed = (middle * scale * gains).astype(BF16)
         for q in range(4):

time: 96.1 us -> 91.6 us (0.953)
  the two profiles are of different devices: /device:TPU:33 before, /device:TPU:1 now
where the time goes in v3:
time: 91.6 us; the launch traced here: 91.5 us
  Pallas kernels  90.7 us (99%)
    pallas_call x1, Pallas kernels, shards(): pl.pallas_call(kernel, out_shape=pltpu.VMEM((ROWS, D), BF16), in_specs=[f...  90.7 us

profile of v3, /device:TPU:1, one launch (start us, length us, event | category | flops | bytes accessed | tf_op | source)
XLA Modules:
  0.0 91.5 jit_solution(8578808302932273760)
XLA Ops:
  0.0 90.7 %layer.1 = bf16[128,2048]{1,0:T(8,128)(2,1)S(1)} custom-call(bf16[128,2048]{1,0:T(8,128)(2,1)} %stream_far.1, bf16[512,256]{1,0:T(8,128)(2,1)} %cia_far.1, bf16[512,256]{1,0:T(8,128)(2,1)} %cib_far.1, bf16[512,256]{1,0:T(8,128)(2,1)} %gia_far.1, bf16[512,256]{1,0:T(8,128)(2,1)} %gib_far.1, bf16[4,256]{1,0:T(4,128)(2,1)} %cwa_far.1, bf16[4,256]{1,0:T(4,128)(2,1)} %cwb_far.1, ...), custom_call_target="tpu_custom_call" | custom-call | tf_op jit(solution)/shard_map/layer/pallas_call | solution.py:590
  90.8 0.8 copy.25

commit v4 on v3

--- a/solution.py
+++ b/solution.py
@@ -1,3 +1,5 @@
+import random
+
 import jax
 import jax.numpy as jnp
 from jax import lax
@@ -39,6 +41,24 @@
     near = w - 1.0
     log1p = jnp.where(near == 0.0, y, jnp.log(w) * (y / jnp.where(near == 0.0, 1.0, near)))
     return jnp.maximum(-d, 0.0) + log1p
+
+
+def hops(step):
+    return -sum(min(n, 4 - n) for n in (step[0], step[1], step[3]))
+
+
+def class_steps(c, seed):
+    steps = []
+    for j in range(32):
+        dc, dx, dy = j % 2, (j // 2) % 4, j // 8
+        steps.append((j, ((c - dx - dy) % 4, dy, dc, dx)))
+    steps = [s for s in steps if any(s[1])]
+    random.Random(seed).shuffle(steps)
+    return steps
+
+
+SENDS = [class_steps(c, c + 1) for c in range(4)]
+REPLIES = [class_steps(c, c + 77) for c in range(4)]
 
 
 def kernel(
@@ -131,15 +151,13 @@
     cores_at = [core, 1 - core]
     yc_at = [[ys_at[n] + cores_at[m] for m in range(2)] for n in range(4)]
 
-    def class_devices(c, sign):
-        zc = [lax.rem(z + sign * (c - n) + 16, 4) * 8 for n in range(7)]
-        found = []
-        for j in range(32):
-            dc, dx, dy = j % 2, (j // 2) % 4, j // 8
-            spot = zc[dx + dy] + yc_at[(sign * dy) % 4][dc]
-            found.append({"sp": spot, "tp": xs_at[(sign * dx) % 4]})
-        return found
-
+    def peer(step, sign=1):
+        dz, dy, dc, dx = (sign * n for n in step)
+        return {"sp": zs_at[dz % 4] + yc_at[dy % 4][dc % 2], "tp": xs_at[dx % 4]}
+
+    barrier = pltpu.get_barrier_semaphore()
+    for step in sorted((step for steps in SENDS for _, step in steps), key=hops):
+        pl.semaphore_signal(barrier, inc=1, device_id=peer(step), device_id_type=MESH)
     pairs = (
         (cia_far, cia),
         (cib_far, cib),
@@ -169,20 +187,6 @@
     for copy in copies:
         copy.start()
     early, middle_loads, loads = copies[:14], copies[14:16], copies[16:]
-
-    barrier = pltpu.get_barrier_semaphore()
-    for dz in range(4):
-        for dy in range(4):
-            for dc in range(2):
-                spot = zs_at[dz] + yc_at[dy][dc]
-                for dx in range(4):
-                    if dz or dy or dc or dx:
-                        pl.semaphore_signal(
-                            barrier,
-                            inc=1,
-                            device_id={"sp": spot, "tp": xs_at[dx]},
-                            device_id_type=MESH,
-                        )
 
     for load in early:
         load.wait()
@@ -325,17 +329,18 @@
     keys[0] = keys[0].T
     keys[1] = keys[1].T
 
-    def pick_matrix(step, carry):
-        r0 = pl.multiple_of(step * 128, 128)
-        c, lane = step // 4, step % 4
-        rho = (iota((128, 128), 1) + r0).astype(F32)
+    def pick_matrix(c, carry):
         k0, k1, w0, w1 = keys[0], keys[1], keys[2], keys[3]
-        for q in range(4):
-            val = jnp.where(rho == k0 + 4.0 * q, w0, 0.0) + jnp.where(rho == k1 + 4.0 * q, w1, 0.0)
-            gm[step, 128 * q : 128 * q + 128, :] = val.astype(BF16)
-        return carry
-
-    lax.fori_loop(0, 16, pick_matrix, 0)
+        for lane in range(4):
+            rho = (iota((128, 128), 1) + (c * 512 + 128 * lane)).astype(F32)
+            cols = slice(128 * lane, 128 * lane + 128)
+            for q in range(4):
+                val = jnp.where(rho == k0 + 4.0 * q, w0, 0.0)
+                val = val + jnp.where(rho == k1 + 4.0 * q, w1, 0.0)
+                gm[c, 128 * q : 128 * q + 128, cols] = val.astype(BF16)
+        return carry
+
+    lax.fori_loop(0, 4, pick_matrix, 0)
 
     for load in middle_loads:
         load.wait()
@@ -436,23 +441,23 @@
             nq[pl.ds(128 * q + r0, 16), :] = normed[:, 512 * q : 512 * q + 512]
         return carry
 
-    lax.fori_loop(0, 8, norms, 0)
+    lax.fori_loop(0, 8, norms, 0, unroll=4)
 
     def send_class(c, src, dst, sem, sign):
-        for j, peer in enumerate(class_devices(c, sign)):
-            tile = pl.ds(pl.multiple_of(c * 512, 512) + 16 * j, 16)
-            copy = pltpu.make_async_remote_copy(
-                src.at[tile],
-                dst.at[tile],
-                sem.at[0],
-                sem.at[1 + c],
-                device_id=peer,
-                device_id_type=MESH,
-            )
-            if j == 0:
-                pl.when(c > 0)(copy.start)
-            else:
-                copy.start()
+        for n, steps in enumerate(SENDS if sign > 0 else REPLIES):
+
+            @pl.when(c == n)
+            def _(n=n, steps=steps):
+                for j, step in steps:
+                    tile = pl.ds(512 * n + 16 * j, 16)
+                    pltpu.make_async_remote_copy(
+                        src.at[tile],
+                        dst.at[tile],
+                        sem.at[0],
+                        sem.at[1 + n],
+                        device_id=peer(step, sign),
+                        device_id_type=MESH,
+                    ).start()
 
     def dispatch(c, carry):
         for n in range(4):
@@ -469,6 +474,11 @@
         load.wait()
 
     def wait_class(buf, sem, c):
+        if isinstance(c, int):
+            part = buf.at[pl.ds(c * 512, 512)]
+            pltpu.make_async_copy(part, part, sem.at[1 + c]).wait()
+            return
+
         @pl.when(c == 0)
         def _():
             part = buf.at[pl.ds(16, 496)]
@@ -510,18 +520,18 @@
 
     def combine(c, carry):
         wait_class(retb, rsem, c)
+        got = pl.ds(pl.multiple_of(c * 512, 512), 512)
         for n in range(4):
             rows = slice(128 * n, 128 * n + 128)
-            part = acc[rows, :]
-            for lane in range(4):
-                r0 = pl.multiple_of(c * 512, 512) + 128 * lane
-                part = part + dot(gm[4 * c + lane, rows, :], retb[pl.ds(r0, 128), :])
-            acc[rows, :] = part
-        return carry
-
-    lax.fori_loop(0, 4, combine, 0)
+            acc[rows, :] = acc[rows, :] + dot(gm[c, rows, :], retb[got, :])
+        return carry
+
+    lax.fori_loop(0, 3, combine, 0)
+    wait_class(retb, rsem, 3)
     for q in range(4):
-        out[:, 512 * q : 512 * q + 512] = acc[128 * q : 128 * q + 128, :].astype(BF16)
+        rows = slice(128 * q, 128 * q + 128)
+        total = acc[rows, :] + dot(gm[3, rows, :], retb[1536:2048, :])
+        out[:, 512 * q : 512 * q + 512] = total.astype(BF16)
 
     pltpu.make_async_copy(told, told, csem.at[0]).wait()
     for copy in sums:
@@ -614,7 +624,7 @@
             V((ROWS, D), F32),
             V((512, Q), BF16),
             V((2048, 512), BF16),
-            V((16, 512, 128), BF16),
+            V((4, 512, 512), BF16),
             V((2048, Q), BF16),
             V((2048, Q), BF16),
             V((2048, Q), BF16),

time: 91.6 us -> 90 us (0.983)
  Pallas kernels: 90.7 us -> 89.1 us
    pallas_call x1, Pallas kernels: 90.7 us -> 89.1 us  [shards(): pl.pallas_call(kernel, out_shape=pltpu.VMEM((ROWS, D), BF16), in_specs=[f...]
where the time goes in v4:
time: 90 us
  Pallas kernels  89.1 us (99%)
    pallas_call x1, Pallas kernels, shards(): pl.pallas_call(kernel, out_shape=pltpu.VMEM((ROWS, D), BF16), in_specs=[f...  89.1 us

profile of v4, /device:TPU:1, one launch (start us, length us, event | category | flops | bytes accessed | tf_op | source)
XLA Modules:
  0.0 90.0 jit_solution(10831129928045005746)
XLA Ops:
  0.0 89.1 %layer.1 = bf16[128,2048]{1,0:T(8,128)(2,1)S(1)} custom-call(bf16[128,2048]{1,0:T(8,128)(2,1)} %stream_far.1, bf16[512,256]{1,0:T(8,128)(2,1)} %cia_far.1, bf16[512,256]{1,0:T(8,128)(2,1)} %cib_far.1, bf16[512,256]{1,0:T(8,128)(2,1)} %gia_far.1, bf16[512,256]{1,0:T(8,128)(2,1)} %gib_far.1, bf16[4,256]{1,0:T(4,128)(2,1)} %cwa_far.1, bf16[4,256]{1,0:T(4,128)(2,1)} %cwb_far.1, ...), custom_call_target="tpu_custom_call" | custom-call | tf_op jit(solution)/shard_map/layer/pallas_call | solution.py:600
  89.2 0.8 copy.25

commit v5 on v4

--- a/solution.py
+++ b/solution.py
@@ -209,13 +209,12 @@
 
     plus = softplus_neg(jnp.concatenate([da[...], db[...]], axis=1)) * GATE_SCALE
 
-    def chunk(step):
-        r0 = pl.multiple_of(step * 64, 64)
-        jump = incb[pl.ds(r0, 64), :]
+    def chunk(r0, size):
+        jump = incb[pl.ds(r0, size), :]
         jump = jnp.concatenate([jump, jump], axis=1)
         for side, taps in enumerate((cwa, cwb)):
             lanes = slice(256 * side, 256 * side + 256)
-            window = xs[pl.ds(r0, 72), lanes]
+            window = xs[pl.ds(r0, size + 8), lanes]
             tap = taps[...].astype(F32)
             total = tap[0:1] * pltpu.roll(window, 3, 0)[8:]
             total = total + tap[1:2] * pltpu.roll(window, 2, 0)[8:]
@@ -229,19 +228,19 @@
             gone = one_minus_square(log, a)
             root = gone * lax.rsqrt(jnp.maximum(gone, 1e-37))
             h = root * admit * conv.astype(F32)
-            a3, h3 = a.reshape(8, 8, 256), h.reshape(8, 8, 256)
-            at = iota((8, 8, 256), 1)
+            a3, h3 = a.reshape(-1, 8, 256), h.reshape(-1, 8, 256)
+            at = iota((size // 8, 8, 256), 1)
             for s in (1, 2, 4):
                 ok = at >= s
                 ap = jnp.where(ok, pltpu.roll(a3, s, 1), 1.0)
                 hp = jnp.where(ok, pltpu.roll(h3, s, 1), 0.0)
                 h3 = h3 + a3 * hp
                 a3 = a3 * ap
-            a8[pl.ds(r0, 64), lanes] = a3.reshape(64, 256)
-            h8[pl.ds(r0, 64), lanes] = h3.reshape(64, 256)
+            a8[pl.ds(r0, size), lanes] = a3.reshape(size, 256)
+            h8[pl.ds(r0, size), lanes] = h3.reshape(size, 256)
 
     def later_chunks(step, carry):
-        chunk(7 - step)
+        chunk(pl.multiple_of((7 - step) * 64, 64), 64)
         return carry
 
     lax.fori_loop(0, 4, later_chunks, 0)
@@ -261,33 +260,42 @@
     for copy in halos:
         copy.start()
 
-    lax.fori_loop(4, 7, later_chunks, 0)
+    lax.fori_loop(4, 8, later_chunks, 0)
+
+    def slab(r0, prod, state):
+        a, h = a8[pl.ds(r0, 8), :], h8[pl.ds(r0, 8), :]
+        h = h + a * state
+        a = a * prod
+        a8[pl.ds(r0, 8), :] = a
+        h8[pl.ds(r0, 8), :] = h
+        return a[7:8], h[7:8]
+
+    def link(step, carry):
+        prod, state = carry
+        for n in range(8):
+            prod, state = slab(pl.multiple_of(step * 64, 64) + 8 * n, prod, state)
+        return prod, state
+
+    prod, state = jnp.ones((1, CH), F32), jnp.zeros((1, CH), F32)
+    for n in range(1, 8):
+        prod, state = slab(8 * n, prod, state)
+    prod, state = lax.fori_loop(1, 8, link, (prod, state))
 
     for copy in halos:
         copy.wait()
     keep = jnp.where(sp > 0, 1.0, 0.0)
     xs[0:8, 0:256] = halo[0].astype(F32)[8:16] * keep
     xs[0:8, 256:512] = halo[1].astype(F32)[8:16] * keep
-    chunk(0)
-
-    def link(step, carry):
-        prod, state = carry
-        for n in range(8):
-            r0 = pl.multiple_of(step * 64, 64) + 8 * n
-            a, h = a8[pl.ds(r0, 8), :], h8[pl.ds(r0, 8), :]
-            h = h + a * state
-            a = a * prod
-            a8[pl.ds(r0, 8), :] = a
-            h8[pl.ds(r0, 8), :] = h
-            prod, state = a[7:8], h[7:8]
-        return prod, state
-
-    prod, state = lax.fori_loop(0, 8, link, (jnp.ones((1, CH), F32), jnp.zeros((1, CH), F32)))
+    chunk(0, 8)
+    head_prod, head_state = a8[7:8, :], h8[7:8, :]
+    state = state + prod * head_state
+    prod = prod * head_prod
+
     for n in range(4):
         stat[n : n + 1, :] = prod[:, 128 * n : 128 * n + 128]
         stat[4 + n : 5 + n, :] = state[:, 128 * n : 128 * n + 128]
 
-    for k in range(1, SPN):
+    for k in sorted(range(1, SPN), key=lambda k: -(min(k // 8, 4 - k // 8) + min(k // 2 % 4, 4 - k // 2 % 4))):
         pltpu.make_async_remote_copy(
             stat,
             carry_in.at[k],
@@ -359,6 +367,10 @@
     for k in range(SPN - 1, 0, -1):
         enter = jnp.where(k <= sp, carry_in[k, 0:4] * enter + carry_in[k, 4:8], enter)
     enter = jnp.concatenate([enter[n : n + 1] for n in range(4)], axis=1)
+
+    h8[0:8, :] = h8[0:8, :] + a8[0:8, :] * enter
+    a8[0:8, :] = jnp.zeros((8, CH), F32)
+    enter = head_state + head_prod * enter
 
     def hiddens(step, carry):
         r0 = pl.multiple_of(lax.rem(step + 2 * x + 4, 8) * 64, 64)

time: 90 us -> 89.2 us (level)
  no operation moved by 1% of the time
where the time goes in v5:
time: 89.2 us; the launch traced here: 89.1 us
  Pallas kernels  88.3 us (99%)
    pallas_call x1, Pallas kernels, shards(): pl.pallas_call(kernel, out_shape=pltpu.VMEM((ROWS, D), BF16), in_specs=[f...  88.3 us

profile of v5, /device:TPU:1, one launch (start us, length us, event | category | flops | bytes accessed | tf_op | source)
XLA Modules:
  0.0 89.1 jit_solution(9950136348329731086)
XLA Ops:
  0.0 88.3 %layer.1 = bf16[128,2048]{1,0:T(8,128)(2,1)S(1)} custom-call(bf16[128,2048]{1,0:T(8,128)(2,1)} %stream_far.1, bf16[512,256]{1,0:T(8,128)(2,1)} %cia_far.1, bf16[512,256]{1,0:T(8,128)(2,1)} %cib_far.1, bf16[512,256]{1,0:T(8,128)(2,1)} %gia_far.1, bf16[512,256]{1,0:T(8,128)(2,1)} %gib_far.1, bf16[4,256]{1,0:T(4,128)(2,1)} %cwa_far.1, bf16[4,256]{1,0:T(4,128)(2,1)} %cwb_far.1, ...), custom_call_target="tpu_custom_call" | custom-call | tf_op jit(solution)/shard_map/layer/pallas_call | solution.py:612
  88.3 0.8 copy.25
